TPU v7x, 32 devices: a whole 2x2x4 slice. The times are simulated.
32 devices in a mesh: sp: 4 (over z), fs: 4 (over y, x), tp: 2 (over core).
Axes of the slice: x: 2, y: 2, z: 4, core: 2. Of those that a mesh axis runs over, the one named last changes fastest.
Arguments:
- activations: bfloat16 [2048, 4096], P(('fs', 'sp'), 'tp'), parts along dimension 0, may hold values from -6 to 6
- input_norm_gain: float32 [4096], replicated, may hold values from 0.1 to 1.9
- window_query_weight: bfloat16 [4096, 2048], P('sp', 'tp'), may hold values from -0.09375 to 0.09375
- window_key_weight: bfloat16 [4096, 512], P('sp', 'tp'), may hold values from -0.09375 to 0.09375
- window_value_weight: bfloat16 [4096, 512], P('sp', 'tp'), may hold values from -0.09375 to 0.09375
- linear_query_weight: bfloat16 [4096, 1024], P('sp', 'tp'), may hold values from -0.09375 to 0.09375
- linear_key_weight: bfloat16 [4096, 1024], P('sp', 'tp'), may hold values from -0.09375 to 0.09375
- linear_value_weight: bfloat16 [4096, 2048], P('sp', 'tp'), may hold values from -0.09375 to 0.09375
- decay_down_factor: bfloat16 [4096, 16], replicated, may hold values from -0.09375 to 0.09375
- decay_up_factor: bfloat16 [16, 1024], P(None, 'tp'), may hold values from -1.5 to 1.5
- decay_offset_bias: float32 [1024], P('tp'), may hold values from -0.5 to 9
- extra_fading_exponent: float32 [2048, 8], P(('fs', 'sp'), 'tp'), parts along dimension 0, may hold values from -1.5 to 0
- starting_state: float32 [8, 128, 256], P('tp'), may hold values from -12 to 12
- head_sink_logit: float32 [32], P('tp'), may hold values from 1 to 5
- linear_head_gain: float32 [256], replicated, may hold values from 0.1 to 1.9
- window_output_weight: bfloat16 [2048, 4096], P('tp', 'sp'), may hold values from -0.09375 to 0.09375
- linear_output_weight: bfloat16 [2048, 4096], P('tp', 'sp'), may hold values from -0.09375 to 0.09375
Outputs:
- mixer_output: bfloat16 [2048, 4096], P(('fs', 'sp', 'tp')), parts along dimension 0
There are 4 independent parts, one for each index of `fs`. A program takes and returns all parts, laid end to end along the dimension named above; an argument that names none is the same for every part. Nothing has to cross between parts.
All inputs are finite; a program needn't handle non-finite values.
Results may differ from a plain program's by a relative error of at most 0.019.
Values may be sent and summed in bfloat16 or wider, within the bound.
A program may use at most 128 MiB of HBM per device.

v0:
```python
import jax
import jax.numpy as jnp
from jax import lax
from jax.sharding import PartitionSpec as P

QH = 32
HD = 64
WINDOW = 128
LOOKUP_FEATURES = 128
DV = 256
SPAN = 64


EPS = 1e-05
FADING_SOFTNESS = 16.0
HIGH_PRECISION = lax.Precision.HIGHEST


def passed_along(value, axis, steps):
    count = lax.axis_size(axis)
    leading, last = (max(0, -steps), min(count, count - steps))
    return lax.ppermute(value, axis, [(source, source + steps) for source in range(leading, last)])


def prefix(x, axis, combine, identity):
    peers, place = (lax.axis_size(axis), lax.axis_index(axis))
    everything = jax.tree.map(
        lambda part, kind: lax.all_gather(part.astype(kind), axis), x, (jnp.bfloat16, jnp.bfloat16)
    )
    start = jax.tree.map(
        lambda part, zero: jnp.broadcast_to(jnp.asarray(zero, part.dtype), part.shape), x, identity
    )

    def hop(k, before):
        reached = k < place
        new = combine(
            before, jax.tree.map(lambda part, own: part[k].astype(own.dtype), everything, x)
        )
        return jax.tree.map(lambda a, b: jnp.where(reached, a, b), new, before)

    return lax.fori_loop(0, peers, hop, start)


def window_attention(near_query, near_keys, near_values, head_sink_logit):
    stream_extent = near_query.shape[0]
    key_heads = near_keys.shape[1] // HD
    heads_here = near_query.shape[1] // HD
    groups = heads_here // key_heads
    blocks = stream_extent // WINDOW
    tail_rows = jnp.stack([near_keys, near_values])
    before = passed_along(tail_rows, "sp", 1)

    def banded(previous, current):
        extended = jnp.concatenate([previous, current], axis=0)
        earlier = extended[:stream_extent].reshape(blocks, WINDOW, key_heads, HD)
        present = extended[WINDOW:].reshape(blocks, WINDOW, key_heads, HD)
        return jnp.concatenate([earlier, present], axis=1)

    key_band = banded(before[0], near_keys)
    value_band = banded(before[1], near_values)
    queries = near_query.reshape(blocks, WINDOW, key_heads, groups, HD)
    scores = jnp.einsum(
        "nqhgd,nkhd->hgnqk", queries, key_band, preferred_element_type=jnp.float32
    ) * HD ** (-0.5)
    head_ids = lax.axis_index("tp") * heads_here + jnp.arange(heads_here, dtype=jnp.int32)
    slopes = jnp.exp2(-8.0 * (head_ids + 1).astype(jnp.float32) / QH).reshape(key_heads, groups)
    query_pos = jnp.arange(WINDOW, dtype=jnp.int32)
    key_pos = jnp.arange(2 * WINDOW, dtype=jnp.int32)
    distance = query_pos[:, None] - key_pos[None, :] + WINDOW
    start_pos = (
        lax.axis_index("sp") * stream_extent + (jnp.arange(blocks, dtype=jnp.int32) - 1) * WINDOW
    )
    absolute = start_pos[:, None] + key_pos[None, :]
    allowed = ((distance >= 0) & (distance < WINDOW))[None] & (absolute >= 0)[:, None, :]
    biased = scores - slopes[:, :, None, None, None] * distance.astype(jnp.float32)
    weights = jnp.where(allowed, jnp.exp(biased), 0.0)
    denominator = (
        jnp.sum(weights, axis=-1, keepdims=True)
        + jnp.exp(head_sink_logit.reshape(key_heads, groups))[:, :, None, None, None]
    )
    attention = (weights / denominator).astype(jnp.bfloat16)
    attended = jnp.einsum(
        "hgnqk,nkhd->nqhgd", attention, value_band, preferred_element_type=jnp.float32
    )
    return attended.reshape(stream_extent, heads_here * HD).astype(jnp.bfloat16)


def linear_attention(
    gated_query, gated_keys, gated_values, fading_exponent, linear_head_gain, starting_state
):
    stream_extent = gated_query.shape[0]
    head_total = gated_query.shape[1] // LOOKUP_FEATURES
    span_count = stream_extent // SPAN
    scaled_query = gated_query.astype(jnp.float32).reshape(
        span_count, SPAN, head_total, LOOKUP_FEATURES
    ) * LOOKUP_FEATURES ** (-0.5)
    keys_wide = gated_keys.astype(jnp.float32).reshape(
        span_count, SPAN, head_total, LOOKUP_FEATURES
    )
    values_wide = gated_values.astype(jnp.float32).reshape(span_count, SPAN, head_total, DV)
    running = jnp.cumsum(
        fading_exponent.reshape(span_count, SPAN, head_total, LOOKUP_FEATURES), axis=1
    )
    span_end = running[:, -1]
    query_with_decay = scaled_query * jnp.exp(running)
    inverse_keys = keys_wide * jnp.exp(-running)
    ending_keys = keys_wide * jnp.exp(span_end[:, None] - running)
    inner = jnp.einsum("nchk,nshk->nhcs", query_with_decay, inverse_keys, precision=HIGH_PRECISION)
    lower = jnp.tril(jnp.ones((SPAN, SPAN), dtype=bool))
    inner = jnp.where(lower, inner, 0.0)
    within = jnp.einsum("nhcs,nshv->nchv", inner, values_wide, precision=HIGH_PRECISION)

    def advance(running_state, inputs):
        query_portion, key_portion, value_portion, scale_factor = inputs
        layer_output = jnp.einsum(
            "fmy,mys->fms", query_portion, running_state, precision=HIGH_PRECISION
        )
        running_state = running_state * scale_factor[..., None] + jnp.einsum(
            "gxp,gxz->xpz", key_portion, value_portion, precision=HIGH_PRECISION
        )
        return (running_state, layer_output)

    start_state = jnp.zeros((head_total, LOOKUP_FEATURES, DV), jnp.float32)
    state_end, carried = lax.scan(
        advance, start_state, (query_with_decay, ending_keys, values_wide, jnp.exp(span_end))
    )
    device_decay = jnp.exp(jnp.sum(span_end, axis=0))
    prefix_sums = jnp.cumsum(span_end, axis=0) - span_end

    def combine(earlier, later):
        return (earlier[0] * later[0], later[0][..., None] * earlier[1] + later[1])

    decay_before, state_before = prefix(
        (device_decay, state_end),
        "sp",
        combine,
        (jnp.ones_like(device_decay), jnp.zeros_like(state_end)),
    )
    incoming_rows = state_before + decay_before[..., None] * starting_state
    crossing = jnp.einsum(
        "qwso,soz->qwsz",
        query_with_decay * jnp.exp(prefix_sums)[:, None],
        incoming_rows,
        precision=HIGH_PRECISION,
    )
    flat = (within + carried + crossing).reshape(stream_extent, head_total, DV)
    normal = (
        flat * lax.rsqrt(jnp.mean(flat * flat, axis=-1, keepdims=True) + EPS) * linear_head_gain
    )
    return normal.reshape(stream_extent, head_total * DV).astype(jnp.bfloat16)


def local(
    activations,
    input_norm_gain,
    window_query_weight,
    window_key_weight,
    window_value_weight,
    linear_query_weight,
    linear_key_weight,
    linear_value_weight,
    decay_down_factor,
    decay_up_factor,
    decay_offset_bias,
    extra_fading_exponent,
    starting_state,
    head_sink_logit,
    linear_head_gain,
    window_output_weight,
    linear_output_weight,
):
    gathered = lax.all_gather(activations, "tp", axis=1, tiled=True)
    widened = gathered.astype(jnp.float32)
    normed = (
        widened
        * lax.rsqrt(jnp.mean(widened * widened, axis=1, keepdims=True) + EPS)
        * input_norm_gain
    ).astype(jnp.bfloat16)
    row_total = normed.shape[0]
    matrices = (
        window_query_weight,
        window_key_weight,
        window_value_weight,
        linear_query_weight,
        linear_key_weight,
        linear_value_weight,
    )
    segments = (
        lax.all_gather(matrices[0], "sp", axis=0, tiled=True),
        lax.all_gather(matrices[1], "sp", axis=0, tiled=True),
        lax.all_gather(matrices[2], "sp", axis=0, tiled=True),
        lax.all_gather(matrices[3], "sp", axis=0, tiled=True),
        lax.all_gather(matrices[4], "sp", axis=0, tiled=True),
        lax.all_gather(matrices[5], "sp", axis=0, tiled=True),
    )
    projected = tuple(
        (jnp.dot(normed, segment, preferred_element_type=jnp.float32) for segment in segments)
    )
    near_query, near_keys, near_values, gated_query, gated_keys, gated_values = [
        product.astype(jnp.bfloat16) for product in projected
    ]
    low_rank = jnp.dot(normed, decay_down_factor, preferred_element_type=jnp.float32).astype(
        jnp.bfloat16
    )
    attention_energies = (
        jnp.dot(low_rank, decay_up_factor, preferred_element_type=jnp.float32) + decay_offset_bias
    )
    head_total = extra_fading_exponent.shape[1]
    fading_exponent = (jax.nn.log_sigmoid(attention_energies) / FADING_SOFTNESS).reshape(
        row_total, head_total, LOOKUP_FEATURES
    ) + extra_fading_exponent[:, :, None]
    near_out = window_attention(near_query, near_keys, near_values, head_sink_logit)
    gated_out = linear_attention(
        gated_query, gated_keys, gated_values, fading_exponent, linear_head_gain, starting_state
    )
    window_full, linear_full = (
        lax.all_gather(window_output_weight, "sp", axis=1, tiled=True),
        lax.all_gather(linear_output_weight, "sp", axis=1, tiled=True),
    )
    return lax.psum_scatter(
        (
            jnp.dot(near_out, window_full, preferred_element_type=jnp.float32)
            + jnp.dot(gated_out, linear_full, preferred_element_type=jnp.float32)
        ).astype(jnp.bfloat16),
        "tp",
        scatter_dimension=0,
        tiled=True,
    )


def solution(mesh):
    placed = (
        P(("fs", "sp"), "tp"),
        P(),
        P("sp", "tp"),
        P("sp", "tp"),
        P("sp", "tp"),
        P("sp", "tp"),
        P("sp", "tp"),
        P("sp", "tp"),
        P(),
        P(None, "tp"),
        P("tp"),
        P(("fs", "sp"), "tp"),
        P("tp", None, None),
        P("tp"),
        P(),
        P("tp", "sp"),
        P("tp", "sp"),
    )
    return jax.shard_map(
        local, mesh=mesh, in_specs=placed, out_specs=P(("fs", "sp", "tp"), None), check_vma=False
    )
```

profile of v0, /device:TPU:0, one launch (start us, length us, event | category | flops | bytes accessed | tf_op | source)
XLA Modules:
  0.0 922.4 jit_solution(5273713908400685786)
XLA Ops:
  6.5 0.7 all-gather.14.cloned.1.call-update
  7.3 0.7 all-gather.26.cloned.1.call-update
  8.1 0.7 all-gather.28.cloned.1.call-update
  8.8 0.5 all-gather.24.cloned.1.call-update
  9.4 0.5 all-gather.16.cloned.1.call-update
  10.0 0.5 all-gather.18.cloned.1.call-update
  10.5 0.7 all-gather.20.cloned.1.call-update
  11.3 0.7 all-gather.22.cloned.1.call-update
  12.1 0.1 copy.80
  12.2 8.4 all-gather.14.cloned.1.call-done
  20.7 1.5 fusion.13
  22.2 2.1 fusion.31
  24.4 0.1 reshape.212
  24.5 0.2 fusion.36
  24.7 79.4 %all-gather.26.cloned.1.call-done = bf16[4096,512]{1,0:T(8,128)(2,1)} async-done(((bf16[1024,512]{1,0:T(8,128)(2,1)}), bf16[4096,512]{1,0:T(8,128)(2,1)}) %all-gather.26.cloned.1.call-update) | async-done | bytes 4194320 | tf_op jit(solution)/shard_map/all_gather | solution.py:192
  104.2 3.0 fusion.23
  107.2 77.8 %all-gather.28.cloned.1.call-done = bf16[4096,512]{1,0:T(8,128)(2,1)} async-done(((bf16[1024,512]{1,0:T(8,128)(2,1)}), bf16[4096,512]{1,0:T(8,128)(2,1)}) %all-gather.28.cloned.1.call-update) | async-done | bytes 4194320 | tf_op jit(solution)/shard_map/all_gather | solution.py:193
  185.0 2.9 fusion.21
  188.1 0.9 exponential_multiply_fusion.1
  189.1 145.5 %all-gather.24.cloned.1.call-done = bf16[4096,1024]{1,0:T(8,128)(2,1)} async-done(((bf16[1024,1024]{1,0:T(8,128)(2,1)}), bf16[4096,1024]{1,0:T(8,128)(2,1)}) %all-gather.24.cloned.1.call-update) | async-done | bytes 8388624 | tf_op jit(solution)/shard_map/all_gather | solution.py:194
  334.6 4.7 convolution_convert_fusion
  339.3 0.2 reshape.211
  339.5 3.8 while.29
  339.5 1.1 fusion.87
  340.7 0.7 convolution_add_fusion.4
  341.4 1.1 fusion.87
  342.6 0.7 convolution_add_fusion.4
  343.4 0.8 convert_element_type.128
  344.2 0.5 all-gather.30.cloned.1.call-update
  345.0 0.1 fusion.48
  345.1 34.8 %all-gather.16.cloned.1.call-done = bf16[4096,256]{1,0:T(8,128)(2,1)} async-done(((bf16[1024,256]{1,0:T(8,128)(2,1)}), bf16[4096,256]{1,0:T(8,128)(2,1)}) %all-gather.16.cloned.1.call-update) | async-done | bytes 2097168 | tf_op jit(solution)/shard_map/all_gather | solution.py:190
  379.9 2.1 convolution_convert_fusion.6
  382.0 43.8 %all-gather.18.cloned.1.call-done = bf16[4096,256]{1,0:T(8,128)(2,1)} async-done(((bf16[1024,256]{1,0:T(8,128)(2,1)}), bf16[4096,256]{1,0:T(8,128)(2,1)}) %all-gather.18.cloned.1.call-update) | async-done | bytes 2097168 | tf_op jit(solution)/shard_map/all_gather | solution.py:191
  425.8 2.1 convolution_convert_fusion.5
  427.9 2.1 collective-permute-start
  430.0 9.4 %all-gather.2 = bf16[4,4,128]{2,1,0:T(4,128)(2,1)S(1)} all-gather(bf16[1,4,128]{2,1,0:T(4,128)(2,1)S(1)} %fusion.50), channel_id=2, replica_groups=mesh['sp'=4,'fs'=4,'tp'=2] {'sp'}, dimensions={0}, use_global_device_ids=true | all-gather | bytes 5120 | tf_op jit(solution)/shard_map/all_gather | solution.py:28
  439.4 0.1 copy.63
  439.5 0.1 copy.61
  439.7 0.1 copy.62
  439.8 0.1 copy.60
  439.9 1.3 convolution_select_fusion
  441.2 134.7 %all-gather.20.cloned.1.call-done = bf16[4096,1024]{1,0:T(8,128)(2,1)} async-done(((bf16[1024,1024]{1,0:T(8,128)(2,1)}), bf16[4096,1024]{1,0:T(8,128)(2,1)}) %all-gather.20.cloned.1.call-update) | async-done | bytes 8388624 | tf_op jit(solution)/shard_map/all_gather | solution.py:189
  575.8 4.7 convolution_convert_fusion.2
  580.5 0.2 copy.64
  580.7 0.8 fusion.64
  581.6 0.3 convolution_convert_fusion.1
  581.9 143.3 %all-gather.22.cloned.1.call-done = bf16[1024,4096]{1,0:T(8,128)(2,1)} async-done(((bf16[1024,1024]{1,0:T(8,128)(2,1)}), bf16[1024,4096]{1,0:T(8,128)(2,1)}) %all-gather.22.cloned.1.call-update) | async-done | bytes 8388624 | tf_op jit(solution)/shard_map/all_gather | solution.py:217
  725.2 4.7 fusion.65
  729.9 23.1 %all-gather.32.cloned.1.call-done = bf16[16,128,256]{2,1,0:T(8,128)(2,1)} async-done(((bf16[4,128,256]{2,1,0:T(8,128)(2,1)}), bf16[16,128,256]{2,1,0:T(8,128)(2,1)}) %all-gather.32.cloned.1.call-update) | async-done | bytes 1048592 | tf_op jit(solution)/shard_map/all_gather | solution.py:28
  753.0 4.8 while.30
  753.0 1.2 fusion.88
  754.3 1.1 fusion.88
  755.5 1.1 fusion.88
  756.7 1.1 fusion.88
  757.9 1.8 convolution_bitcast_fusion.1
  759.7 1.4 multiply_reduce_fusion
  761.2 0.1 copy.81
  761.3 0.2 mul.189
  761.5 0.1 copy.85
  761.6 0.3 copy.74
  761.9 0.1 copy.84
  762.0 141.4 %all-gather.30.cloned.1.call-done = bf16[1024,4096]{1,0:T(8,128)(2,1)} async-done(((bf16[1024,1024]{1,0:T(8,128)(2,1)}), bf16[1024,4096]{1,0:T(8,128)(2,1)}) %all-gather.30.cloned.1.call-update) | async-done | bytes 8388624 | tf_op jit(solution)/shard_map/all_gather | solution.py:218
  903.4 5.7 fusion.12
  909.1 6.7 reduce-scatter.2.cloned.1.call-done
  (75 shorter events, 1.2 us)
Async XLA Ops:
  6.5 15.7 %copy-start = (bf16[4096,16]{0,1:T(8,128)(2,1)S(1)}, bf16[4096,16]{0,1:T(8,128)(2,1)}, u32[]{:S(2)}) copy-start(bf16[4096,16]{0,1:T(8,128)(2,1)} %param.29) | copy-start | bytes 393220
  6.5 14.1 %all-gather.14.cloned.1.call-start = ((), (), s32[]{:S(2)}) async-start(), calls=%async_computation.1 | async-start | bytes 1572864 | tf_op jit(solution)/shard_map/all_gather | solution.py:172
  7.3 96.9 %all-gather.26.cloned.1.call-start = ((), (), s32[]{:S(2)}) async-start(), calls=%async_computation.7 | async-start | bytes 5242880 | tf_op jit(solution)/shard_map/all_gather | solution.py:192
  8.0 177.0 %all-gather.28.cloned.1.call-start = ((), (), s32[]{:S(2)}) async-start(), calls=%async_computation.8 | async-start | bytes 5242880 | tf_op jit(solution)/shard_map/all_gather | solution.py:193
  8.7 325.9 %all-gather.24.cloned.1.call-start = ((), (), s32[]{:S(2)}) async-start(), calls=%async_computation.6 | async-start | bytes 10485760 | tf_op jit(solution)/shard_map/all_gather | solution.py:194
  9.3 370.6 %all-gather.16.cloned.1.call-start = ((), (), s32[]{:S(2)}) async-start(), calls=%async_computation.2 | async-start | bytes 2621440 | tf_op jit(solution)/shard_map/all_gather | solution.py:190
  9.9 415.9 %all-gather.18.cloned.1.call-start = ((), (), s32[]{:S(2)}) async-start(), calls=%async_computation.3 | async-start | bytes 2621440 | tf_op jit(solution)/shard_map/all_gather | solution.py:191
  10.5 1.6 copy-start.5
  10.5 565.3 %all-gather.20.cloned.1.call-start = ((), (), s32[]{:S(2)}) async-start(), calls=%async_computation.4 | async-start | bytes 10485760 | tf_op jit(solution)/shard_map/all_gather | solution.py:189
  11.2 11.0 %copy-start.7 = (bf16[16,512]{1,0:T(8,128)(2,1)S(1)}, bf16[16,512]{1,0:T(8,128)(2,1)}, u32[]{:S(2)}) copy-start(bf16[16,512]{1,0:T(8,128)(2,1)} %param.30) | copy-start | bytes 49156
  11.3 11.0 %copy-start.8 = (f32[4096]{0:T(1024)S(1)}, f32[4096]{0:T(1024)}, u32[]{:S(2)}) copy-start(f32[4096]{0:T(1024)} %param.22) | copy-start | bytes 49156
  11.3 11.0 %copy-start.10 = (f32[512]{0:T(512)S(1)}, f32[512]{0:T(512)}, u32[]{:S(2)}) copy-start(f32[512]{0:T(512)} %param.31) | copy-start | bytes 6148
  11.3 714.0 %all-gather.22.cloned.1.call-start = ((), (), s32[]{:S(2)}) async-start(), calls=%async_computation.5 | async-start | bytes 10485760 | tf_op jit(solution)/shard_map/all_gather | solution.py:217
  12.0 741.0 %all-gather.32.cloned.1.call-start = ((), (), s32[]{:S(2)}) async-start(), calls=%async_computation.11 | async-start | bytes 1310720 | tf_op jit(solution)/shard_map/all_gather | solution.py:28
  22.2 82.0 %copy-start.2 = (bf16[128,4096]{1,0:T(8,128)(2,1)S(1)}, bf16[128,4096]{1,0:T(8,128)(2,1)}, u32[]{:S(2)}) copy-start(bf16[128,4096]{1,0:T(8,128)(2,1)} %all-gather.14.cloned.1.call-done) | copy-start | bytes 3145732
  343.3 1.5 copy-start.11
  343.4 1.6 copy-start.6
  343.4 36.5 %copy-start.9 = (f32[4096]{0:T(1024)S(1)}, f32[4096]{0:T(1024)}, u32[]{:S(2)}) copy-start(f32[4096]{0:T(1024)} %param.22) | copy-start | bytes 49156
  344.2 559.3 %all-gather.30.cloned.1.call-start = ((), (), s32[]{:S(2)}) async-start(), calls=%async_computation.9 | async-start | bytes 10485760 | tf_op jit(solution)/shard_map/all_gather | solution.py:218
  344.8 571.1 %reduce-scatter.2.cloned.1.call-start = ((), (), s32[]{:S(2)}) async-start(), calls=%async_computation.10 | async-start | bytes 1572864 | tf_op jit(solution)/shard_map/reduce_scatter | solution.py:220
  427.9 11.7 %collective-permute-start = (bf16[2,128,256]{2,1,0:T(8,128)(2,1)S(1)}, bf16[2,128,256]{2,1,0:T(8,128)(2,1)S(1)}, u32[]{:S(2)}, u32[]{:S(2)}) collective-permute-start(bf16[2,128,256]{2,1,0:T(8,128)(2,1)S(1)} %pad_maximum_fusion), channel_id=1, source_target_pairs={{0,8},{8,16},{16,24},{1,9},{9,17},{17,25},{2,10},{10,18},{18,26},{... | collective-permute-start | bytes 393224 | tf_op jit(solution)/shard_map/ppermute | solution.py:22
  753.0 4.9 copy-start.3
  757.9 1.8 copy-start.4
  903.4 12.4 %copy-start.1 = (bf16[4096,16]{0,1:T(8,128)(2,1)S(1)}, bf16[4096,16]{0,1:T(8,128)(2,1)}, u32[]{:S(2)}) copy-start(bf16[4096,16]{0,1:T(8,128)(2,1)} %param.29) | copy-start | bytes 393220
Sparse Core Ops, SparseCore 0:
  8.9 11.7 all-gather.13
  22.2 81.9 all-gather.25
  105.7 79.2 all-gather.27
  186.5 148.0 all-gather.23
  336.0 43.8 all-gather.15
  381.3 44.4 all-gather.17
  427.4 148.3 all-gather.19
  577.4 147.7 all-gather.21
  726.8 26.1 all-gather.31
  754.4 148.9 all-gather.29
  909.3 6.5 reduce-scatter.1
where the time goes:
time: 923 us; the launch traced here: 922 us
  waiting for transfers between devices  845 us (92%)
  matrix products  41.2 us (4%)
  between operations  13.7 us (1%)
  blocking collectives  9.38 us (1%)
    all_gather x1, waiting for transfers between devices, local(): lax.all_gather(matrices[5], 'sp', axis=0, tiled=True)  146 us
    all_gather x1, waiting for transfers between devices, local(): lax.all_gather(window_output_weight, 'sp', axis=1, tiled=True)  143 us
    all_gather x1, waiting for transfers between devices, local(): lax.all_gather(linear_output_weight, 'sp', axis=1, tiled=True)  141 us
    all_gather x1, waiting for transfers between devices, local(): lax.all_gather(matrices[0], 'sp', axis=0, tiled=True)  135 us
    all_gather x1, waiting for transfers between devices, local(): lax.all_gather(matrices[3], 'sp', axis=0, tiled=True)  79.4 us
    all_gather x1, waiting for transfers between devices, local(): lax.all_gather(matrices[4], 'sp', axis=0, tiled=True)  77.8 us
    all_gather x1, waiting for transfers between devices, local(): lax.all_gather(matrices[2], 'sp', axis=0, tiled=True)  43.8 us
    all_gather x1, waiting for transfers between devices, local(): lax.all_gather(matrices[1], 'sp', axis=0, tiled=True)  34.8 us
  transfers between devices with their start and end apart: 12, of which 11 were waited for; matrix products, arithmetic and copies ran while one was open for 5% of the time, Pallas kernels for 0%

commit v1 on v0

--- a/solution.py
+++ b/solution.py
@@ -9,6 +9,8 @@
 LOOKUP_FEATURES = 128
 DV = 256
 SPAN = 64
+KVH = 8
+GATED_MIXERS = 8
 
 
 EPS = 1e-05
@@ -228,6 +230,170 @@
     )
 
 
+def head_window(near_query, near_keys, near_values, head_sink_logit, first_head):
+    stream_extent = near_query.shape[0]
+    key_heads = near_keys.shape[1] // HD
+    heads_here = near_query.shape[1] // HD
+    groups = heads_here // key_heads
+    blocks = stream_extent // WINDOW
+
+    def banded(current):
+        extended = jnp.concatenate(
+            [jnp.zeros((WINDOW, current.shape[1]), current.dtype), current], axis=0
+        )
+        earlier = extended[:stream_extent].reshape(blocks, WINDOW, key_heads, HD)
+        present = extended[WINDOW:].reshape(blocks, WINDOW, key_heads, HD)
+        return jnp.concatenate([earlier, present], axis=1)
+
+    key_band = banded(near_keys)
+    value_band = banded(near_values)
+    queries = near_query.reshape(blocks, WINDOW, key_heads, groups, HD)
+    scores = jnp.einsum(
+        "nqhgd,nkhd->hgnqk", queries, key_band, preferred_element_type=jnp.float32
+    ) * HD ** (-0.5)
+    head_ids = first_head + jnp.arange(heads_here, dtype=jnp.int32)
+    slopes = jnp.exp2(-8.0 * (head_ids + 1).astype(jnp.float32) / QH).reshape(key_heads, groups)
+    query_pos = jnp.arange(WINDOW, dtype=jnp.int32)
+    key_pos = jnp.arange(2 * WINDOW, dtype=jnp.int32)
+    distance = query_pos[:, None] - key_pos[None, :] + WINDOW
+    absolute = (jnp.arange(blocks, dtype=jnp.int32) - 1)[:, None] * WINDOW + key_pos[None, :]
+    allowed = ((distance >= 0) & (distance < WINDOW))[None] & (absolute >= 0)[:, None, :]
+    biased = scores - slopes[:, :, None, None, None] * distance.astype(jnp.float32)
+    weights = jnp.where(allowed, jnp.exp(biased), 0.0)
+    denominator = (
+        jnp.sum(weights, axis=-1, keepdims=True)
+        + jnp.exp(head_sink_logit.reshape(key_heads, groups))[:, :, None, None, None]
+    )
+    attention = (weights / denominator).astype(jnp.bfloat16)
+    attended = jnp.einsum(
+        "hgnqk,nkhd->nqhgd", attention, value_band, preferred_element_type=jnp.float32
+    )
+    return attended.reshape(stream_extent, heads_here * HD).astype(jnp.bfloat16)
+
+
+def head_linear(gated_query, gated_keys, gated_values, fading, gain, state):
+    stream_extent = gated_query.shape[0]
+    heads = gated_query.shape[1] // LOOKUP_FEATURES
+    spans = stream_extent // SPAN
+    bf = jnp.bfloat16
+
+    def mm(spec, a, b):
+        return jnp.einsum(spec, a.astype(bf), b.astype(bf), preferred_element_type=jnp.float32)
+
+    queries = gated_query.astype(jnp.float32).reshape(
+        spans, SPAN, heads, LOOKUP_FEATURES
+    ) * LOOKUP_FEATURES ** (-0.5)
+    keys = gated_keys.astype(jnp.float32).reshape(spans, SPAN, heads, LOOKUP_FEATURES)
+    values = gated_values.reshape(spans, SPAN, heads, DV)
+    running = jnp.cumsum(fading.reshape(spans, SPAN, heads, LOOKUP_FEATURES), axis=1)
+    span_end = running[:, -1]
+    decayed = queries * jnp.exp(running)
+    inner = mm("nchk,nshk->nhcs", decayed, keys * jnp.exp(-running))
+    inner = jnp.where(jnp.tril(jnp.ones((SPAN, SPAN), dtype=bool)), inner, 0.0)
+    within = mm("nhcs,nshv->nchv", inner, values)
+    added = mm("nshk,nshv->nhkv", keys * jnp.exp(span_end[:, None] - running), values)
+    scale = jnp.exp(span_end)
+    before = []
+    for n in range(spans):
+        before.append(state)
+        state = state * scale[n][..., None] + added[n]
+    carried = mm("nchk,nhkv->nchv", decayed, jnp.stack(before))
+    flat = within + carried
+    normal = flat * lax.rsqrt(jnp.mean(flat * flat, axis=-1, keepdims=True) + EPS) * gain
+    return normal.reshape(stream_extent, heads * DV).astype(bf)
+
+
+def stationary(
+    activations,
+    input_norm_gain,
+    window_query_weight,
+    window_key_weight,
+    window_value_weight,
+    linear_query_weight,
+    linear_key_weight,
+    linear_value_weight,
+    decay_down_factor,
+    decay_up_factor,
+    decay_offset_bias,
+    extra_fading_exponent,
+    starting_state,
+    head_sink_logit,
+    linear_head_gain,
+    window_output_weight,
+    linear_output_weight,
+):
+    bf = jnp.bfloat16
+    sp, tp = lax.axis_size("sp"), lax.axis_size("tp")
+    me_sp, me_tp = lax.axis_index("sp"), lax.axis_index("tp")
+    rows = activations.shape[0]
+    tokens = rows * sp
+    gathered = lax.all_gather(activations, "tp", axis=1, tiled=True)
+    widened = gathered.astype(jnp.float32)
+    normed = (
+        widened
+        * lax.rsqrt(jnp.mean(widened * widened, axis=1, keepdims=True) + EPS)
+        * input_norm_gain
+    ).astype(bf)
+    low_own = jnp.dot(normed, decay_down_factor, preferred_element_type=jnp.float32).astype(bf)
+    low_rank = lax.all_gather(low_own, "sp", axis=0, tiled=True)
+    fade_own = lax.all_to_all(extra_fading_exponent, "sp", 1, 0, tiled=True)
+    slices = lax.all_to_all(normed, "sp", 1, 0, tiled=True)
+    matrices = (
+        window_query_weight,
+        window_key_weight,
+        window_value_weight,
+        linear_query_weight,
+        linear_key_weight,
+        linear_value_weight,
+    )
+    parts = [
+        jnp.dot(slices, m, preferred_element_type=jnp.float32)
+        .astype(bf)
+        .reshape(tokens, sp, m.shape[1] // sp)
+        .transpose(1, 0, 2)
+        for m in matrices
+    ]
+    widths = [m.shape[1] // sp for m in matrices]
+    joined = lax.psum_scatter(jnp.concatenate(parts, axis=2), "sp", scatter_dimension=0)
+    pieces, at = [], 0
+    for width in widths:
+        pieces.append(joined[:, at : at + width])
+        at += width
+    near_query, near_keys, near_values, gated_query, gated_keys, gated_values = pieces
+    heads = fade_own.shape[1]
+    channels = heads * LOOKUP_FEATURES
+    up = lax.dynamic_slice_in_dim(decay_up_factor, me_sp * channels, channels, 1)
+    bias = lax.dynamic_slice_in_dim(decay_offset_bias, me_sp * channels, channels, 0)
+    energies = jnp.dot(low_rank, up, preferred_element_type=jnp.float32) + bias
+    fading = (jax.nn.log_sigmoid(energies) / FADING_SOFTNESS).reshape(
+        tokens, heads, LOOKUP_FEATURES
+    ) + fade_own[:, :, None]
+    near_heads = near_query.shape[1] // HD
+    sinks = lax.dynamic_slice_in_dim(head_sink_logit, me_sp * near_heads, near_heads, 0)
+    near_out = head_window(
+        near_query, near_keys, near_values, sinks, (me_tp * sp + me_sp) * near_heads
+    )
+    state = lax.dynamic_slice_in_dim(starting_state, me_sp * heads, heads, 0)
+    gated_out = head_linear(
+        gated_query, gated_keys, gated_values, fading, linear_head_gain, state
+    )
+    both = lax.all_gather(jnp.concatenate([near_out, gated_out], axis=1), "sp", axis=0)
+    split = near_out.shape[1]
+    near_full = both[:, :, :split].transpose(1, 0, 2).reshape(tokens, -1)
+    gated_full = both[:, :, split:].transpose(1, 0, 2).reshape(tokens, -1)
+    term = (
+        jnp.dot(near_full, window_output_weight, preferred_element_type=jnp.float32)
+        + jnp.dot(gated_full, linear_output_weight, preferred_element_type=jnp.float32)
+    ).astype(bf)
+    term = term.reshape(sp, tp, rows // tp, -1)
+    summed = lax.psum_scatter(term, "tp", scatter_dimension=1)
+    return lax.all_to_all(summed, "sp", 0, 2, tiled=True).reshape(rows // tp, -1)
+
+
+def divides(sp, tp):
+    return GATED_MIXERS % (sp * tp) == 0 and KVH % (sp * tp) == 0 and QH % (sp * tp) == 0
+
+
 def solution(mesh):
     placed = (
         P(("fs", "sp"), "tp"),
@@ -248,6 +414,7 @@
         P("tp", "sp"),
         P("tp", "sp"),
     )
+    body = stationary if divides(mesh.shape["sp"], mesh.shape["tp"]) else local
     return jax.shard_map(
-        local, mesh=mesh, in_specs=placed, out_specs=P(("fs", "sp", "tp"), None), check_vma=False
-    )
+        body, mesh=mesh, in_specs=placed, out_specs=P(("fs", "sp", "tp"), None), check_vma=False
+    )

time: 923 us -> 283 us (0.31)
  waiting for transfers between devices: 845 us -> 120 us
  blocking collectives: 9.38 us -> 63.5 us
  local copies, waits for them, and re-layouts: 2.26 us -> 45.5 us
  matrix products: 41.2 us -> 23.1 us
    all_gather x10 -> x2, waiting for transfers between devices: 832 us -> 57.6 us  [the longest x1 45.8 us: stationary(): lax.all_gather(jnp.concatenate([near_out, gated_out], axis=1), 'sp', axis=0)]
    all_to_all x0 -> x2, blocking collectives: none -> 50.6 us  [the longest x1 31 us: stationary(): slices = lax.all_to_all(normed, 'sp', 1, 0, tiled=True)]
    reduce_scatter x1, waiting for transfers between devices: 6.7 us -> 44.7 us  [stationary(): lax.psum_scatter(jnp.concatenate(parts, axis=2), 'sp', scatter_dimension=0)]
    dot_general x18 -> x15, matrix products: 41.2 us -> 23.1 us  [the longest x6 14.2 us: stationary(): jnp.dot(slices, m, preferred_element_type=jnp.float32).astype(bf)]
    unnamed x11 -> x5, waiting for transfers between devices: 5.62 us -> 17.9 us
  transfers between devices with their start and end apart: 12 -> 5, of which waited for: 11 -> 4; matrix products, arithmetic and copies ran while one was open for 5% -> 3% of each run, Pallas kernels for 0% -> 0%
where the time goes in v1:
time: 283 us; the launch traced here: 281 us
  waiting for transfers between devices  120 us (42%)
  blocking collectives  63.5 us (22%)
  local copies, waits for them, and re-layouts  45.5 us (16%)
  matrix products  23.1 us (8%)
  between operations  13.5 us (5%)
  other arithmetic  11.8 us (4%)
  starting transfers between devices  3.67 us (1%)
    all_gather x1, waiting for transfers between devices, stationary(): lax.all_gather(jnp.concatenate([near_out, gated_out], axis=1), 'sp', axis=0)  45.8 us
    reduce_scatter x1, waiting for transfers between devices, stationary(): lax.psum_scatter(jnp.concatenate(parts, axis=2), 'sp', scatter_dimension=0)  44.7 us
    all_to_all x1, blocking collectives, stationary(): slices = lax.all_to_all(normed, 'sp', 1, 0, tiled=True)  31 us
    all_to_all x1, blocking collectives, stationary(): lax.all_to_all(summed, 'sp', 0, 2, tiled=True).reshape(rows // tp, -1)  19.6 us
    unnamed x5, waiting for transfers between devices  17.9 us
    dot_general x6, matrix products, stationary(): jnp.dot(slices, m, preferred_element_type=jnp.float32).astype(bf)  14.2 us
    all_gather x1, blocking collectives, stationary(): low_rank = lax.all_gather(low_own, 'sp', axis=0, tiled=True)  12.9 us
    all_gather x1, waiting for transfers between devices, stationary(): gathered = lax.all_gather(activations, 'tp', axis=1, tiled=True)  11.9 us
  transfers between devices with their start and end apart: 5, of which 4 were waited for; matrix products, arithmetic and copies ran while one was open for 3% of the time, Pallas kernels for 0%

profile of v1, /device:TPU:0, one launch (start us, length us, event | category | flops | bytes accessed | tf_op | source)
XLA Modules:
  0.0 281.3 jit_solution(11022463948495590396)
XLA Ops:
  6.5 2.2 copy.118
  8.8 11.9 %all-gather.4.cloned.1.call-done = bf16[128,4096]{0,1:T(8,128)(2,1)} async-done(((bf16[128,2048]{0,1:T(8,128)(2,1)}), bf16[128,4096]{0,1:T(8,128)(2,1)}) %all-gather.4.cloned.1.call-update) | async-done | bytes 1048592 | tf_op jit(solution)/shard_map/all_gather | solution.py:330
  20.7 1.8 fusion
  22.5 1.7 fusion.2
  24.2 31.0 %all_to_all.50 = bf16[128,4,1024]{0,2,1:T(8,128)(2,1)} all-to-all(bf16[128,4,1024]{0,2,1:T(8,128)(2,1)S(1)} %bitcast.158), channel_id=1, replica_groups=mesh['sp'=4,'fs'=4,'tp'=2] {'sp'}, dimensions={1} | all-to-all | bytes 2097152 | tf_op jit(solution)/shard_map/all_to_all | solution.py:340
  55.2 2.3 copy.119
  57.4 3.6 %convolution_convert_fusion.1 = bf16[512,1024]{1,0:T(8,128)(2,1)} fusion(bf16[512,1024]{1,0:T(8,128)(2,1)} %bitcast.159, bf16[1024,1024]{1,0:T(8,128)(2,1)S(1)} %copy-done), kind=kOutput, calls=%fused_computation.11 | convolution fusion | flops 1074266112 | bytes 4194304 | tf_op jit(solution)/shard_map/dot_general | solution.py:350
  61.0 2.3 convolution_convert_fusion
  63.3 1.6 convolution_convert_fusion.2
  64.9 2.1 copy.124
  66.9 3.1 %convolution_convert_fusion.3 = bf16[512,512]{0,1:T(8,128)(2,1)} fusion(bf16[512,1024]{1,0:T(8,128)(2,1)} %bitcast.160, bf16[1024,512]{1,0:T(8,128)(2,1)} %param.22), kind=kOutput, calls=%fused_computation.13 | convolution fusion | flops 537133056 | bytes 2621440 | tf_op jit(solution)/shard_map/dot_general | solution.py:350
  70.0 2.0 copy.123
  72.1 1.8 convolution_convert_fusion.6
  73.9 1.0 copy.121
  74.9 1.8 convolution_convert_fusion.5
  76.7 1.0 copy.122
  77.7 3.0 %bitcast_bitcast_fusion = (bf16[4,512,256]{2,1,0:T(8,128)(2,1)}, bf16[4,512,256]{2,1,0:T(8,128)(2,1)}) fusion(bf16[64,4,8,256]{3,2,1,0:T(8,128)(2,1)} %bitcast.190, bf16[64,4,8,256]{3,2,1,0:T(8,128)(2,1)} %bitcast.189), kind=kLoop, calls=%fused_computation.25 | loop fusion | bytes 4194304 | tf_op jit(solution)/shard_map/transpose | solution.py:353
  80.8 6.8 %concatenate.22 = bf16[4,512,896]{2,1,0:T(8,128)(2,1)} concatenate(bf16[4,512,256]{2,1,0:T(8,128)(2,1)} %get-tuple-element.34, bf16[4,512,64]{2,1,0:T(8,128)(2,1)} %bitcast.173, bf16[4,512,64]{2,1,0:T(8,128)(2,1)} %bitcast.174, bf16[4,512,128]{2,1,0:T(8,128)(2,1)} %bitcast.172, bf16[4,512,128]{2,1,0:T(8,128)(2,1)} %bitcast.171, bf16[4,512,256]{2,1,0:T(8,128)(2,1)} %get-tuple-element.33), dimensions={2} | concatenate | bytes 7340032 | tf_op jit(solution)/shard_map/concatenate | solution.py:357
  87.6 3.4 %all-to-all-start.1 = ((f32[128,4,1]{0,2,1:T(1,128)}), f32[128,4,1]{0,2,1:T(1,128)S(1)}, u32[]{:S(2)}, u32[]{:S(2)}) async-start(f32[128,4,1]{0,2,1:T(1,128)} %bitcast.31), calls=%async_computation.2 | async-start | bytes 4096 | tf_op jit(solution)/shard_map/all_to_all | solution.py:339
  91.1 0.8 dynamic_slice.14
  91.8 0.7 dynamic-slice_exponential_fusion
  92.5 1.6 fusion.43
  94.2 0.9 broadcast_and_fusion
  95.1 0.9 broadcast_multiply_fusion
  96.0 0.2 convolution_convert_fusion.7
  96.3 12.9 %all_gather.13 = bf16[512,16]{0,1:T(8,128)(2,1)S(1)} all-gather(bf16[128,16]{0,1:T(8,128)(2,1)S(1)} %convolution_convert_fusion.7), channel_id=1, replica_groups=mesh['sp'=4,'fs'=4,'tp'=2] {'sp'}, dimensions={0}, use_global_device_ids=true | all-gather | bytes 20480 | tf_op jit(solution)/shard_map/all_gather | solution.py:338
  109.2 1.0 fusion.13
  110.4 0.6 slice_bitcast_fusion.1
  111.0 44.7 %reduce-scatter.5.cloned.1.call-done = bf16[1,512,896]{2,1,0:T(8,128)(2,1)} async-done(((bf16[4,512,896]{2,1,0:T(8,128)(2,1)}), bf16[1,512,896]{2,1,0:T(8,128)(2,1)}) %reduce-scatter.5.cloned.1.call-update) | async-done | bytes 917520 | tf_op jit(solution)/shard_map/reduce_scatter | solution.py:357
  155.7 1.1 fusion.51
  156.8 1.1 fusion.52
  157.8 0.9 slice.118
  158.8 0.9 convert_multiply_fusion.2
  159.7 0.7 pad_slice_fusion
  160.4 1.6 copy.132
  162.0 0.7 copy.133
  162.7 1.1 reshape.392
  163.8 0.7 copy.128
  164.6 2.0 fusion.57
  166.7 0.3 fusion.6
  167.1 0.2 copy.137
  167.3 0.7 copy.197
  168.1 1.0 fusion.18
  169.1 0.3 fusion.29
  169.5 1.0 convert_dynamic-update-slice_fusion.5
  171.1 0.2 fusion.39
  171.4 1.3 multiply_reduce_fusion
  172.7 0.8 multiply_convert_fusion
  173.7 1.8 pad_maximum_fusion
  175.5 0.2 all-reduce.5.cloned.1.call-start
  175.7 45.8 %all-gather.6.cloned.1.call-done = bf16[2048,512]{0,1:T(8,128)(2,1)} async-done(((bf16[512,512]{0,1:T(8,128)(2,1)}), bf16[2048,512]{0,1:T(8,128)(2,1)}) %all-gather.6.cloned.1.call-update) | async-done | bytes 2097168 | tf_op jit(solution)/shard_map/all_gather | solution.py:380
  221.5 4.5 %reshape.389 = bf16[4,512,512]{1,0,2:T(4,128)(2,1)} reshape(bf16[2048,512]{0,1:T(8,128)(2,1)} %all-gather.6.cloned.1.call-done) | data formatting | bytes 4194304 | tf_op jit(solution)/shard_map/all_gather | solution.py:380
  226.0 2.3 fusion.50
  228.2 0.2 copy.165
  228.7 1.2 copy-done.2
  229.8 1.3 fusion.58
  231.1 0.3 copy-done.15
  231.4 2.2 add_convert_fusion
  233.7 0.6 dynamic-slice
  234.3 17.8 %all-reduce.5.cloned.1.call-done = bf16[4,2,64,1024]{3,2,1,0:T(8,128)(2,1)} async-done(((bf16[4,2,64,1024]{3,2,1,0:T(8,128)(2,1)}), bf16[4,2,64,1024]{3,2,1,0:T(8,128)(2,1)}) %all-reduce.5.cloned.1.call-update) | async-done | bytes 1048592
  252.1 1.7 dynamic-slice_bitcast_fusion
  253.8 19.6 %all_to_all.51 = bf16[4,64,1024]{2,1,0:T(8,128)(2,1)S(1)} all-to-all(bf16[4,64,1024]{2,1,0:T(8,128)(2,1)S(1)} %dynamic-slice_bitcast_fusion), channel_id=1, replica_groups=mesh['sp'=4,'fs'=4,'tp'=2] {'sp'}, dimensions={0} | all-to-all | bytes 1048576 | tf_op jit(solution)/shard_map/all_to_all | solution.py:390
  273.4 0.4 copy.149
  273.8 1.0 copy.170
  (66 shorter events, 1.7 us)
Async XLA Ops:
  6.5 50.9 %copy-start = (bf16[1024,1024]{1,0:T(8,128)(2,1)S(1)}, bf16[1024,1024]{1,0:T(8,128)(2,1)}, u32[]{:S(2)}) copy-start(bf16[1024,1024]{1,0:T(8,128)(2,1)} %param.19) | copy-start | bytes 6291460
  6.5 15.9 %copy-start.6 = (f32[4096]{0:T(1024)S(1)}, f32[4096]{0:T(1024)}, u32[]{:S(2)}) copy-start(f32[4096]{0:T(1024)} %param.18) | copy-start | bytes 49156
  6.5 14.1 %all-gather.4.cloned.1.call-start = ((), (), s32[]{:S(2)}) async-start(), calls=%async_computation.4 | async-start | bytes 1572864 | tf_op jit(solution)/shard_map/all_gather | solution.py:330
  8.8 146.9 %reduce-scatter.5.cloned.1.call-start = ((), (), s32[]{:S(2)}) async-start(), calls=%async_computation.5 | async-start | bytes 4587520 | tf_op jit(solution)/shard_map/reduce_scatter | solution.py:357
  57.4 3.6 %copy-start.1 = (bf16[4,128,1024]{2,1,0:T(8,128)(2,1)S(1)}, bf16[4,128,1024]{2,1,0:T(8,128)(2,1)}, u32[]{:S(2)}) copy-start(bf16[4,128,1024]{2,1,0:T(8,128)(2,1)} %copy.119) | copy-start | bytes 3145732
  57.4 3.6 %copy-start.14 = (bf16[1024,1024]{1,0:T(8,128)(2,1)S(1)}, bf16[1024,1024]{1,0:T(8,128)(2,1)}, u32[]{:S(2)}) copy-start(bf16[1024,1024]{1,0:T(8,128)(2,1)} %param.24) | copy-start | bytes 6291460
  61.0 2.3 copy-start.16
  87.6 4.2 %copy-start.17 = (f32[16]{0:T(128)S(1)}, f32[16]{0:T(128)}, u32[]{:S(2)}) copy-start(f32[16]{0:T(128)} %param.30) | copy-start | bytes 196
  87.6 8.4 %copy-start.4 = (bf16[4096,16]{0,1:T(8,128)(2,1)S(1)}, bf16[4096,16]{0,1:T(8,128)(2,1)}, u32[]{:S(2)}) copy-start(bf16[4096,16]{0,1:T(8,128)(2,1)} %param.25) | copy-start | bytes 393220
  87.6 21.5 %all-to-all-start.1 = ((f32[128,4,1]{0,2,1:T(1,128)}), f32[128,4,1]{0,2,1:T(1,128)S(1)}, u32[]{:S(2)}, u32[]{:S(2)}) async-start(f32[128,4,1]{0,2,1:T(1,128)} %bitcast.31), calls=%async_computation.2 | async-start | bytes 4096 | tf_op jit(solution)/shard_map/all_to_all | solution.py:339
  91.0 130.5 %all-gather.6.cloned.1.call-start = ((), (), s32[]{:S(2)}) async-start(), calls=%async_computation.6 | async-start | bytes 2621440 | tf_op jit(solution)/shard_map/all_gather | solution.py:380
  164.5 2.1 copy-start.13
  164.5 2.2 copy-start.5
  167.0 2.4 copy-start.3
  167.1 2.4 copy-start.12
  167.3 3.2 %copy-start.8 = (f32[128]{0:T(128)S(1)}, f32[128]{0:T(128)}, u32[]{:S(2)}) copy-start(f32[128]{0:T(128)} %get-tuple-element.27) | copy-start | bytes 1540
  167.3 3.3 %copy-start.11 = (f32[128]{0:T(128)S(1)}, f32[128]{0:T(128)}, u32[]{:S(2)}) copy-start(f32[128]{0:T(128)} %get-tuple-element.26) | copy-start | bytes 1540
  168.1 2.6 copy-start.7
  168.1 2.7 copy-start.10
  169.1 1.9 copy-start.9
  175.5 76.6 %all-reduce.5.cloned.1.call-start = ((), (), s32[]{:S(2)}) async-start(), calls=%async_computation.7 | async-start | bytes 2097152
  228.2 1.6 copy-start.2
  229.8 1.6 copy-start.15
  231.4 2.3 copy-start.18
Sparse Core Ops, SparseCore 0:
  8.9 11.7 all-gather.3
  87.7 67.8 reduce-scatter.4
  175.6 45.8 all-gather.5
  233.8 18.2 all-reduce.4

commit v2 on v1

--- a/solution.py
+++ b/solution.py
@@ -1,6 +1,10 @@
+import functools
+
 import jax
 import jax.numpy as jnp
 from jax import lax
+from jax.experimental import pallas as pl
+from jax.experimental.pallas import tpu as pltpu
 from jax.sharding import PartitionSpec as P
 
 QH = 32
@@ -303,6 +307,345 @@
     return normal.reshape(stream_extent, heads * DV).astype(bf)
 
 
+MESH = pl.DeviceIdType.MESH
+BF = jnp.bfloat16
+F32 = jnp.float32
+
+
+def dot(a, b):
+    return jnp.dot(a, b, preferred_element_type=F32)
+
+
+def remote(src, dst, send_sem, recv_sem, **where):
+    return pltpu.make_async_remote_copy(
+        src_ref=src,
+        dst_ref=dst,
+        send_sem=send_sem,
+        recv_sem=recv_sem,
+        device_id=where,
+        device_id_type=MESH,
+    )
+
+
+def greet(sp, tp):
+    s, t = lax.axis_index("sp"), lax.axis_index("tp")
+    barrier = pltpu.get_barrier_semaphore()
+    for ds in range(sp):
+        for dt in range(tp):
+            if ds or dt:
+                where = {"sp": lax.rem(s + ds, sp), "tp": lax.rem(t + dt, tp)}
+                pl.semaphore_signal(barrier, inc=1, device_id=where, device_id_type=MESH)
+    pl.semaphore_wait(barrier, sp * tp - 1)
+
+
+def project_kernel(sp, tp, widths, *refs):
+    x, gain, down, fade = refs[:4]
+    sources = refs[4:10]
+    joined, small = refs[10:12]
+    weights = refs[12:18]
+    squares, normed, blocks, note, part, right_in, left_in = refs[18:25]
+    w_sem, sq_sem, a_send, a_recv, f_send, l_sem, n_send, n_recv = refs[25:33]
+    r_send, r_recv, b_send, b_recv = refs[33:37]
+    s, t = lax.axis_index("sp"), lax.axis_index("tp")
+    other = 1 - t
+    per_half = sp // tp
+    rows, half = x.shape
+    width = half // per_half
+    loads = [
+        pltpu.make_async_copy(a, b, w_sem.at[i]) for i, (a, b) in enumerate(zip(sources, weights))
+    ]
+    for load in loads:
+        load.start()
+    wide = x[...].astype(F32)
+    own = jnp.sum(wide * wide, axis=1, keepdims=True)
+    squares[0] = jnp.broadcast_to(own, (rows, 128))
+    greet(sp, tp)
+    swap = remote(squares.at[0], squares.at[1], sq_sem.at[0], sq_sem.at[1], tp=other)
+    swap.start()
+    swap.wait()
+    total = own + squares[1][:, :1]
+    scale = lax.rsqrt(total / (half * tp) + EPS)
+    for i in range(per_half):
+        cols = slice(i * width, (i + 1) * width)
+        normed[i] = (x[:, cols].astype(F32) * scale * gain[t, :, cols]).astype(BF)
+    home = lax.div(s, per_half) == t
+
+    def slice_send(i):
+        j = t * per_half + i
+        return remote(normed.at[i], blocks.at[s], a_send.at[i], a_recv.at[s], sp=j)
+
+    for i in range(per_half):
+
+        @pl.when(t * per_half + i != s)
+        def _():
+            slice_send(i).start()
+
+        @pl.when(t * per_half + i == s)
+        def _():
+            keep = pltpu.make_async_copy(normed.at[i], blocks.at[s], l_sem)
+            keep.start()
+            keep.wait()
+
+    low = jnp.zeros((down.shape[1], rows), F32)
+    for i in range(per_half):
+        low += lax.dot_general(
+            down[t, :, i * width : (i + 1) * width],
+            normed[i],
+            (((1,), (1,)), ((), ())),
+            preferred_element_type=F32,
+        )
+    note[s, t, : down.shape[1]] = low
+    note[s, t, down.shape[1] :] = fade[...]
+
+    def note_send(n):
+        where = {"sp": lax.rem(s + n // tp, sp), "tp": lax.rem(t + n % tp, tp)}
+        return remote(note.at[s, t], note.at[s, t], n_send.at[n], n_recv.at[s, t], **where)
+
+    for n in range(1, sp * tp):
+        note_send(n).start()
+    for load in loads:
+        load.wait()
+
+    def forward(b):
+        return remote(blocks.at[b], blocks.at[b], f_send.at[b], a_recv.at[b], tp=other)
+
+    def right(b, d):
+        return remote(
+            part.at[b, d], right_in.at[b, d], r_send.at[b, d], r_recv.at[b, d], sp=jnp.minimum(s + 1, sp - 1)
+        )
+
+    def left(b, d):
+        return remote(
+            part.at[b, d], left_in.at[b, d], b_send.at[b, d], b_recv.at[b, d], sp=jnp.maximum(s - 1, 0)
+        )
+
+    def compute(k, carry):
+        step = jnp.where(s < (sp + 1) // 2, k, sp - k)
+        b = lax.rem(s + step, sp)
+
+        @pl.when(jnp.logical_or(jnp.logical_not(home), b != s))
+        def _():
+            forward(b).wait_recv()
+
+        @pl.when(home)
+        def _():
+            forward(b).start()
+
+        block = blocks[b]
+        keys = dot(block, weights[1][...])
+        vals = dot(block, weights[2][...])
+
+        def fill(d):
+            at = 0
+            for i, m in enumerate(weights):
+                w = widths[i]
+                if i == 1:
+                    piece = keys[:, d * w : (d + 1) * w]
+                elif i == 2:
+                    piece = vals[:, d * w : (d + 1) * w]
+                else:
+                    piece = dot(block, m[:, d * w : (d + 1) * w])
+                part[b, d, :, at : at + w] = piece.astype(BF)
+                at += w
+
+        for n in range(sp):
+            fill(n)
+
+        @pl.when(s == 0)
+        def _():
+            for d in range(sp - 1, 0, -1):
+                right(b, d).start()
+
+        @pl.when(s == sp - 1)
+        def _():
+            for d in range(sp - 1):
+                left(b, d).start()
+
+        return carry
+
+    lax.fori_loop(0, sp, compute, 0)
+
+    def relay(k, carry):
+        br, bl = k, sp - 1 - k
+        for n in range(sp - 1):
+            dr, dl = sp - 1 - n, n
+
+            @pl.when(jnp.logical_and(s > 0, s < dr))
+            def _():
+                right(br, dr).wait_recv()
+                part[br, dr] = (part[br, dr].astype(F32) + right_in[br, dr].astype(F32)).astype(BF)
+                right(br, dr).start()
+
+            @pl.when(jnp.logical_and(s < sp - 1, s > dl))
+            def _():
+                left(bl, dl).wait_recv()
+                part[bl, dl] = (part[bl, dl].astype(F32) + left_in[bl, dl].astype(F32)).astype(BF)
+                left(bl, dl).start()
+
+        return carry
+
+    lax.fori_loop(0, sp, relay, 0)
+
+    def finish(b, carry):
+        joined[b] = part[b, s]
+
+        @pl.when(s > 0)
+        def _():
+            right(b, s).wait_recv()
+            joined[b] = (joined[b].astype(F32) + right_in[b, s].astype(F32)).astype(BF)
+
+        @pl.when(s < sp - 1)
+        def _():
+            left(b, s).wait_recv()
+            joined[b] = (joined[b].astype(F32) + left_in[b, s].astype(F32)).astype(BF)
+
+        for d in range(sp):
+
+            @pl.when(s < d)
+            def _():
+                right(b, d).wait_send()
+
+            @pl.when(s > d)
+            def _():
+                left(b, d).wait_send()
+
+        @pl.when(home)
+        def _():
+            forward(b).wait_send()
+
+        return carry
+
+    lax.fori_loop(0, sp, finish, 0)
+    for i in range(per_half):
+
+        @pl.when(t * per_half + i != s)
+        def _():
+            slice_send(i).wait_send()
+
+    for n in range(1, sp * tp):
+        note_send(n).wait_send()
+        ps, pt = lax.rem(s + n // tp, sp), lax.rem(t + n % tp, tp)
+        remote(note.at[ps, pt], note.at[ps, pt], n_send.at[n], n_recv.at[ps, pt], tp=other).wait_recv()
+    small[...] = note[...]
+
+
+def output_kernel(sp, tp, order, *refs):
+    near, gated, near_w, gated_w, out = refs[:5]
+    w1, w2, held, term, away, landed = refs[5:11]
+    w_sem, r_send, r_recv, b_send, b_recv, t_send, t_recv, o_send, o_recv = refs[11:20]
+    s, t = lax.axis_index("sp"), lax.axis_index("tp")
+    other = 1 - t
+    rows = held.shape[2]
+    split = near.shape[1]
+    part = rows // tp
+    loads = [
+        pltpu.make_async_copy(near_w, w1, w_sem.at[0]),
+        pltpu.make_async_copy(gated_w, w2, w_sem.at[1]),
+    ]
+    for load in loads:
+        load.start()
+    for b in range(sp):
+        held[b, s, :, :split] = near[b * rows : (b + 1) * rows]
+        held[b, s, :, split:] = gated[b * rows : (b + 1) * rows]
+    greet(sp, tp)
+
+    def right(b, src):
+        ref = held.at[b, src]
+        return remote(ref, ref, r_send.at[b, src], r_recv.at[b, src], sp=jnp.minimum(s + 1, sp - 1))
+
+    def left(b, src):
+        ref = held.at[b, src]
+        return remote(ref, ref, b_send.at[b, src], b_recv.at[b, src], sp=jnp.maximum(s - 1, 0))
+
+    def start_own(b):
+        @pl.when(s < sp - 1)
+        def _():
+            right(b, s).start()
+
+        @pl.when(s > 0)
+        def _():
+            left(b, s).start()
+
+    def swap(b):
+        return remote(term.at[b, other], away.at[b], t_send.at[b], t_recv.at[b], tp=other)
+
+    def deliver(b):
+        return remote(term.at[b, t], landed.at[s], o_send.at[b], o_recv.at[s], sp=b)
+
+    def close(b):
+        swap(b).wait()
+        term[b, t] = (term[b, t].astype(F32) + away[b].astype(F32)).astype(BF)
+
+        @pl.when(s != b)
+        def _():
+            deliver(b).start()
+
+        @pl.when(s == b)
+        def _():
+            landed[b] = term[b, t]
+
+    start_own(order[0])
+    for load in loads:
+        load.wait()
+    for k, b in enumerate(order):
+        if k + 1 < sp:
+            start_own(order[k + 1])
+        for n in range(1, sp):
+
+            @pl.when(s - n >= 0)
+            def _():
+                src = jnp.maximum(s - n, 0)
+                right(b, src).wait_recv()
+
+                @pl.when(s < sp - 1)
+                def _():
+                    right(b, src).start()
+
+            @pl.when(s + n < sp)
+            def _():
+                src = jnp.minimum(s + n, sp - 1)
+                left(b, src).wait_recv()
+
+                @pl.when(s > 0)
+                def _():
+                    left(b, src).start()
+
+        if k:
+            close(order[k - 1])
+        total = None
+        for src in range(sp):
+            block = held[b, src]
+            piece = dot(block[:, :split], w1[src * split : (src + 1) * split]) + dot(
+                block[:, split:], w2[src * (block.shape[1] - split) : (src + 1) * (block.shape[1] - split)]
+            )
+            total = piece if total is None else total + piece
+        for h in range(tp):
+            term[b, h] = total[h * part : (h + 1) * part].astype(BF)
+        swap(b).start()
+    close(order[-1])
+    for b in range(sp):
+        for src in range(sp):
+
+            @pl.when(jnp.logical_and(src <= s, s < sp - 1))
+            def _():
+                right(b, src).wait_send()
+
+            @pl.when(jnp.logical_and(src >= s, s > 0))
+            def _():
+                left(b, src).wait_send()
+
+    for b in range(sp):
+
+        @pl.when(s != b)
+        def _():
+            deliver(b).wait_send()
+            remote(landed.at[b], landed.at[b], o_send.at[b], o_recv.at[b], tp=other).wait_recv()
+
+    columns = landed.shape[2]
+    for b in range(sp):
+        out[:, b * columns : (b + 1) * columns] = landed[b]
+
+
 def stationary(
     activations,
     input_norm_gain,
@@ -322,22 +665,10 @@
     window_output_weight,
     linear_output_weight,
 ):
-    bf = jnp.bfloat16
     sp, tp = lax.axis_size("sp"), lax.axis_size("tp")
     me_sp, me_tp = lax.axis_index("sp"), lax.axis_index("tp")
-    rows = activations.shape[0]
+    rows, half = activations.shape
     tokens = rows * sp
-    gathered = lax.all_gather(activations, "tp", axis=1, tiled=True)
-    widened = gathered.astype(jnp.float32)
-    normed = (
-        widened
-        * lax.rsqrt(jnp.mean(widened * widened, axis=1, keepdims=True) + EPS)
-        * input_norm_gain
-    ).astype(bf)
-    low_own = jnp.dot(normed, decay_down_factor, preferred_element_type=jnp.float32).astype(bf)
-    low_rank = lax.all_gather(low_own, "sp", axis=0, tiled=True)
-    fade_own = lax.all_to_all(extra_fading_exponent, "sp", 1, 0, tiled=True)
-    slices = lax.all_to_all(normed, "sp", 1, 0, tiled=True)
     matrices = (
         window_query_weight,
         window_key_weight,
@@ -346,21 +677,65 @@
         linear_key_weight,
         linear_value_weight,
     )
-    parts = [
-        jnp.dot(slices, m, preferred_element_type=jnp.float32)
-        .astype(bf)
-        .reshape(tokens, sp, m.shape[1] // sp)
-        .transpose(1, 0, 2)
-        for m in matrices
-    ]
-    widths = [m.shape[1] // sp for m in matrices]
-    joined = lax.psum_scatter(jnp.concatenate(parts, axis=2), "sp", scatter_dimension=0)
+    widths = tuple(m.shape[1] // sp for m in matrices)
+    total = sum(widths)
+    rank = decay_down_factor.shape[1]
+    heads_tp = extra_fading_exponent.shape[1]
+    gain = input_norm_gain.reshape(tp, 1, half)
+    down = decay_down_factor.T.reshape(rank, tp, half).transpose(1, 0, 2)
+    fade = jnp.pad(extra_fading_exponent.T, ((0, -heads_tp % 8), (0, 0)))
+    noted = rank + fade.shape[0]
+    vmem = pl.BlockSpec(memory_space=pltpu.VMEM)
+    anywhere = pl.BlockSpec(memory_space=pl.ANY)
+    dma = pltpu.SemaphoreType.DMA
+    joined, small = pl.pallas_call(
+        functools.partial(project_kernel, sp, tp, widths),
+        out_shape=(
+            jax.ShapeDtypeStruct((sp, rows, total), BF),
+            jax.ShapeDtypeStruct((sp, tp, noted, rows), F32),
+        ),
+        in_specs=[vmem] * 4 + [anywhere] * 6,
+        out_specs=(vmem, vmem),
+        scratch_shapes=[pltpu.VMEM(m.shape, BF) for m in matrices]
+        + [
+            pltpu.VMEM((2, rows, 128), F32),
+            pltpu.VMEM((sp // tp, rows, half * tp // sp), BF),
+            pltpu.VMEM((sp, rows, half * tp // sp), BF),
+            pltpu.VMEM((sp, tp, noted, rows), F32),
+            pltpu.VMEM((sp, sp, rows, total), BF),
+            pltpu.VMEM((sp, sp, rows, total), BF),
+            pltpu.VMEM((sp, sp, rows, total), BF),
+            dma((6,)),
+            dma((2,)),
+            dma((sp // tp,)),
+            dma((sp,)),
+            dma((sp,)),
+            dma,
+            dma((sp * tp,)),
+            dma((sp, tp)),
+            dma((sp, sp)),
+            dma((sp, sp)),
+            dma((sp, sp)),
+            dma((sp, sp)),
+        ],
+        compiler_params=pltpu.CompilerParams(
+            collective_id=0, has_side_effects=True, vmem_limit_bytes=48 * 2**20
+        ),
+    )(activations, gain, down, fade, *matrices)
+    joined = joined.reshape(tokens, total)
+    low_rank = (
+        jnp.sum(small[:, :, :rank], axis=1).transpose(0, 2, 1).reshape(tokens, rank).astype(BF)
+    )
+    heads = heads_tp // sp
+    fade_own = lax.dynamic_slice_in_dim(
+        lax.dynamic_index_in_dim(small, me_tp, 1, False), rank + me_sp * heads, heads, 1
+    )
+    fade_own = fade_own.transpose(0, 2, 1).reshape(tokens, heads)
     pieces, at = [], 0
     for width in widths:
         pieces.append(joined[:, at : at + width])
         at += width
     near_query, near_keys, near_values, gated_query, gated_keys, gated_values = pieces
-    heads = fade_own.shape[1]
     channels = heads * LOOKUP_FEATURES
     up = lax.dynamic_slice_in_dim(decay_up_factor, me_sp * channels, channels, 1)
     bias = lax.dynamic_slice_in_dim(decay_offset_bias, me_sp * channels, channels, 0)
@@ -377,21 +752,41 @@
     gated_out = head_linear(
         gated_query, gated_keys, gated_values, fading, linear_head_gain, state
     )
-    both = lax.all_gather(jnp.concatenate([near_out, gated_out], axis=1), "sp", axis=0)
-    split = near_out.shape[1]
-    near_full = both[:, :, :split].transpose(1, 0, 2).reshape(tokens, -1)
-    gated_full = both[:, :, split:].transpose(1, 0, 2).reshape(tokens, -1)
-    term = (
-        jnp.dot(near_full, window_output_weight, preferred_element_type=jnp.float32)
-        + jnp.dot(gated_full, linear_output_weight, preferred_element_type=jnp.float32)
-    ).astype(bf)
-    term = term.reshape(sp, tp, rows // tp, -1)
-    summed = lax.psum_scatter(term, "tp", scatter_dimension=1)
-    return lax.all_to_all(summed, "sp", 0, 2, tiled=True).reshape(rows // tp, -1)
+    columns = window_output_weight.shape[1]
+    both = near_out.shape[1] + gated_out.shape[1]
+    order = sorted(range(sp), key=lambda b: -abs(2 * b - sp + 1))
+    return pl.pallas_call(
+        functools.partial(output_kernel, sp, tp, order),
+        out_shape=jax.ShapeDtypeStruct((rows // tp, columns * sp), BF),
+        in_specs=[vmem] * 2 + [anywhere] * 2,
+        out_specs=vmem,
+        scratch_shapes=[
+            pltpu.VMEM(window_output_weight.shape, BF),
+            pltpu.VMEM(linear_output_weight.shape, BF),
+            pltpu.VMEM((sp, sp, rows, both), BF),
+            pltpu.VMEM((sp, tp, rows // tp, columns), BF),
+            pltpu.VMEM((sp, rows // tp, columns), BF),
+            pltpu.VMEM((sp, rows // tp, columns), BF),
+            dma((2,)),
+            dma((sp, sp)),
+            dma((sp, sp)),
+            dma((sp, sp)),
+            dma((sp, sp)),
+            dma((sp,)),
+            dma((sp,)),
+            dma((sp,)),
+            dma((sp,)),
+        ],
+        compiler_params=pltpu.CompilerParams(
+            collective_id=1, has_side_effects=True, vmem_limit_bytes=48 * 2**20
+        ),
+    )(near_out, gated_out, window_output_weight, linear_output_weight)
 
 
 def divides(sp, tp):
-    return GATED_MIXERS % (sp * tp) == 0 and KVH % (sp * tp) == 0 and QH % (sp * tp) == 0
+    heads = sp * tp
+    fits = GATED_MIXERS % heads == 0 and KVH % heads == 0 and QH % heads == 0
+    return tp == 2 and sp % tp == 0 and fits
 
 
 def solution(mesh):

time: 283 us -> 173 us (0.61)
  Pallas kernels: 0 us -> 150 us
  waiting for transfers between devices: 120 us -> 0 us
  blocking collectives: 63.5 us -> 0 us
  local copies, waits for them, and re-layouts: 45.5 us -> 13.6 us
  matrix products: 23.1 us -> 5.45 us
  between operations: 13.5 us -> 0.35 us
  other arithmetic: 11.8 us -> 2.86 us
  starting transfers between devices: 3.67 us -> 0 us
    pallas_call x0 -> x2, Pallas kernels: none -> 150 us  [the longest x1 96.6 us: stationary(): pl.pallas_call(functools.partial(project_kernel, sp, tp, widths), out_sha...]
    all_gather x2 -> x0, waiting for transfers between devices: 57.6 us -> none  [the longest x1 45.8 us: stationary(): lax.all_gather(jnp.concatenate([near_out, gated_out], axis=1), 'sp', axis=0)]
    all_to_all x2 -> x0, blocking collectives: 50.6 us -> none  [the longest x1 31 us: stationary(): slices = lax.all_to_all(normed, 'sp', 1, 0, tiled=True)]
    reduce_scatter x1 -> x0, waiting for transfers between devices: 44.7 us -> none  [stationary(): lax.psum_scatter(jnp.concatenate(parts, axis=2), 'sp', scatter_dimension=0)]
    dot_general x9 -> x0, matrix products: 17.9 us -> none  [the longest x6 14.2 us: stationary(): jnp.dot(slices, m, preferred_element_type=jnp.float32).astype(bf)]
    unnamed x5 -> x0, waiting for transfers between devices: 17.9 us -> none
    all_gather x1 -> x0, blocking collectives: 12.9 us -> none  [stationary(): low_rank = lax.all_gather(low_own, 'sp', axis=0, tiled=True)]
    concatenate x1 -> x0, local copies, waits for them, and re-layouts: 6.83 us -> none  [stationary(): jnp.concatenate(parts, axis=2)]
  transfers between devices with their start and end apart: 5 -> 0, of which waited for: 4 -> 0; matrix products, arithmetic and copies ran while one was open for 3% -> 0% of each run, Pallas kernels for 0% -> 0%
where the time goes in v2:
time: 173 us; the launch traced here: 172 us
  Pallas kernels  150 us (87%)
  local copies, waits for them, and re-layouts  13.6 us (8%)
  matrix products  5.45 us (3%)
  other arithmetic  2.86 us (2%)
    pallas_call x1, Pallas kernels, stationary(): pl.pallas_call(functools.partial(project_kernel, sp, tp, widths), out_sha...  96.6 us
    pallas_call x1, Pallas kernels, stationary(): pl.pallas_call(functools.partial(output_kernel, sp, tp, order), out_shape...  53.2 us
    unnamed x24, local copies, waits for them, and re-layouts  9.61 us

profile of v2, /device:TPU:0, one launch (start us, length us, event | category | flops | bytes accessed | tf_op | source)
XLA Modules:
  0.0 172.1 jit_solution(17862490236836684599)
XLA Ops:
  0.0 0.0 copy-start
  0.0 0.9 copy.111
  0.9 0.7 pad.6.refs_3_
  1.6 0.0 copy-start.3
  1.6 1.2 copy-done.3
  2.8 0.0 copy-start.4
  2.8 1.2 copy-done.4
  4.1 0.0 copy-start.5
  4.1 1.0 copy-done.5
  5.1 0.0 copy-start.6
  5.1 1.0 copy-done.6
  6.2 0.0 copy-start.7
  6.2 1.0 copy-done.7
  7.2 0.0 copy-start.8
  7.2 0.7 copy-done.8
  7.9 96.6 %shard_map.163 = (bf16[4,128,896]{2,1,0:T(8,128)(2,1)S(1)}, f32[4,2,24,128]{3,2,1,0:T(8,128)S(1)}) custom-call(bf16[128,2048]{1,0:T(8,128)(2,1)S(1)} %copy-done.5, f32[2,1,2048]{2,1,0:T(1,128)S(1)} %bitcast.112, bf16[2,16,2048]{2,1,0:T(8,128)(2,1)S(1)} %bitcast.111, f32[8,128]{1,0:T(8,128)S(1)} %pad.6.refs_3_, bf16[1024,1024]{1,0:T(8,128)(2,1)} %refs_4_.1, ...), custom_call_target="tpu_custom_call" | custom-call | tf_op jit(solution)/shard_map/pallas_call | solution.py:691
  104.6 0.8 dynamic_slice.19
  105.3 0.0 copy-done
  105.3 0.4 fusion.10
  105.7 0.2 fusion.19
  106.0 0.4 fusion.15
  106.4 0.3 fusion.26
  106.8 0.9 fusion.40
  107.7 1.0 convert_dynamic-update-slice_fusion.5
  108.7 0.1 convert_dynamic-update-slice_fusion.4
  108.8 0.1 convert_dynamic-update-slice_fusion.3
  108.9 0.1 convert_dynamic-update-slice_fusion.2
  109.0 0.0 copy-start.9
  109.0 0.1 convert_dynamic-update-slice_fusion.1
  109.1 0.1 convert_dynamic-update-slice_fusion
  109.2 0.1 fusion.41
  109.3 0.2 fusion.36
  109.6 0.4 multiply_reduce_fusion
  110.0 0.0 copy-done.9
  110.0 0.1 multiply_convert_fusion
  110.2 0.1 fusion.50
  110.3 0.1 copy.50
  110.5 0.1 broadcast_multiply_fusion
  110.6 0.1 copy.51
  110.7 0.2 reshape.350
  111.0 0.0 copy-start.10
  111.0 0.1 add_compare_fusion
  111.1 0.2 broadcast_and_fusion
  111.3 2.1 %fusion.51 = (f32[4,4,128]{2,0,1:T(4,128)S(1)}, f32[1,4,4,128,256]{3,4,1,2,0:T(8,128)}) fusion(f32[4,128,256]{1,2,0:T(8,128)S(1)} %broadcast_multiply_fusion, bf16[4,128,4,64]{3,2,1,0:T(4,128)(2,1)S(1)} %reshape.350, bf16[4,128,1,64]{1,3,0,2:T(8,128)(2,1)S(1)} %copy.51, bf16[4,128,1,64]{1,3,0,2:T(8,128)(2,1)S(1)} %copy.50, ...), kind=kOutput, calls=%fused_computation.103 | convolution fusion | flops 69466112 | bytes 3153920 | tf_op jit(solution)/shard_map/nqhgd,nkhd->hgnqk/dot_general | solution.py:255
  113.4 0.0 copy-done.10
  113.4 0.1 dynamic-slice_exponential_fusion
  113.5 0.1 broadcast_add_fusion
  113.5 0.1 copy.46
  113.6 0.1 copy.47
  113.8 0.0 copy-start.1
  113.8 2.1 %fusion.3 = bf16[4,128,1,4,64]{1,4,3,0,2:T(8,128)(2,1)S(1)} fusion(f32[1,4,4,128,256]{3,4,1,2,0:T(8,128)} %get-tuple-element.32, f32[4,4,128]{2,0,1:T(4,128)S(1)} %broadcast_add_fusion, bf16[4,128,1,64]{1,3,0,2:T(8,128)(2,1)S(1)} %copy.47, bf16[4,128,1,64]{1,3,0,2:T(8,128)(2,1)S(1)} %copy.46), kind=kOutput, calls=%fused_computation.8 | convolution fusion | flops 68550656 | bytes 2498560 | tf_op jit(solution)/shard_map/hgnqk,nkhd->nqhgd/dot_general | solution.py:272
  115.8 0.3 copy.79
  116.2 0.3 reshape.351.refs_0_
  116.5 0.0 copy-done.1
  116.5 0.0 copy-start.2
  116.5 1.6 copy-done.2
  118.1 53.2 %shard_map.164 = bf16[64,4096]{1,0:T(8,128)(2,1)S(1)} custom-call(bf16[512,256]{1,0:T(8,128)(2,1)S(1)} %reshape.351.refs_0_, bf16[512,256]{1,0:T(8,128)(2,1)S(1)} %bitcast.110, bf16[1024,1024]{1,0:T(8,128)(2,1)S(1)} %copy-done.1, bf16[1024,1024]{1,0:T(8,128)(2,1)S(1)} %copy-done.2), custom_call_target="tpu_custom_call" | custom-call | tf_op jit(solution)/shard_map/pallas_call | solution.py:758
  171.3 0.8 copy.120
  (15 shorter events, 0.3 us)
Async XLA Ops:
  0.0 105.3 %copy-start = (bf16[16,512]{1,0:T(8,128)(2,1)S(1)}, bf16[16,512]{1,0:T(8,128)(2,1)}, u32[]{:S(2)}) copy-start(bf16[16,512]{1,0:T(8,128)(2,1)} %param.26) | copy-start | bytes 49156
  1.6 1.2 copy-start.3
  2.8 1.2 copy-start.4
  4.1 1.0 copy-start.5
  5.1 1.0 copy-start.6
  6.2 1.0 copy-start.7
  7.2 0.7 copy-start.8
  109.0 1.0 copy-start.9
  111.0 2.4 %copy-start.10 = (f32[16]{0:T(128)S(1)}, f32[16]{0:T(128)}, u32[]{:S(2)}) copy-start(f32[16]{0:T(128)} %param.30) | copy-start | bytes 196
  113.8 2.7 %copy-start.1 = (bf16[1024,1024]{1,0:T(8,128)(2,1)S(1)}, bf16[1024,1024]{1,0:T(8,128)(2,1)}, u32[]{:S(2)}) copy-start(bf16[1024,1024]{1,0:T(8,128)(2,1)} %refs_2_.1) | copy-start | bytes 6291460
  116.5 1.6 copy-start.2

commit v3 on v0

--- a/solution.py
+++ b/solution.py
@@ -1,6 +1,10 @@
+import functools
+
 import jax
 import jax.numpy as jnp
 from jax import lax
+from jax.experimental import pallas as pl
+from jax.experimental.pallas import tpu as pltpu
 from jax.sharding import PartitionSpec as P
 
 QH = 32
@@ -9,6 +13,8 @@
 LOOKUP_FEATURES = 128
 DV = 256
 SPAN = 64
+KVH = 8
+GATED_MIXERS = 8
 
 
 EPS = 1e-05
@@ -228,6 +234,540 @@
     )
 
 
+MESH = pl.DeviceIdType.MESH
+BF = jnp.bfloat16
+F32 = jnp.float32
+
+
+def dot(a, b):
+    return jnp.dot(a, b, preferred_element_type=F32)
+
+
+def remote(src, dst, send_sem, recv_sem, **where):
+    return pltpu.make_async_remote_copy(
+        src_ref=src,
+        dst_ref=dst,
+        send_sem=send_sem,
+        recv_sem=recv_sem,
+        device_id=where,
+        device_id_type=MESH,
+    )
+
+
+def greet(sp, tp):
+    s, t = lax.axis_index("sp"), lax.axis_index("tp")
+    barrier = pltpu.get_barrier_semaphore()
+    for ds in range(sp):
+        for dt in range(tp):
+            if ds or dt:
+                where = {"sp": lax.rem(s + ds, sp), "tp": lax.rem(t + dt, tp)}
+                pl.semaphore_signal(barrier, inc=1, device_id=where, device_id_type=MESH)
+    pl.semaphore_wait(barrier, sp * tp - 1)
+
+
+def columns_dot(a, b):
+    return lax.dot_general(a, b, (((1,), (1,)), ((), ())), preferred_element_type=F32)
+
+
+def mixer_kernel(sp, tp, widths, order, *refs):
+    x, gain, down, fade, up, bias, sink, head_gain = refs[:8]
+    sources, state_in, out = refs[8:16], refs[16], refs[17]
+    weights, start = refs[18:26], refs[26]
+    squares, normed, blocks, note, term, away, landed = refs[27:34]
+    lin = refs[34:38]
+    win = refs[38:42]
+    held_g, held_n = refs[42:44]
+    w_sem, sq_sem, a_send, a_recv, f_send, l_sem, n_send, n_recv = refs[44:52]
+    lin_sem, win_sem, g_sem, h_sem = refs[52:56], refs[56:60], refs[60:64], refs[64:68]
+    t_send, t_recv, o_send, o_recv = refs[68:72]
+    s, t = lax.axis_index("sp"), lax.axis_index("tp")
+    other = 1 - t
+    after, ahead = jnp.minimum(s + 1, sp - 1), jnp.maximum(s - 1, 0)
+    per_half = sp // tp
+    rows, half = x.shape
+    width = half // per_half
+    rank = down.shape[1]
+    loads = [
+        pltpu.make_async_copy(a, b, w_sem.at[i]) for i, (a, b) in enumerate(zip(sources, weights))
+    ]
+    loads.append(pltpu.make_async_copy(state_in.at[s], start, w_sem.at[len(sources)]))
+    for i in (3, 4, 5, 0, 1, 2, 8, 6, 7):
+        loads[i].start()
+    wide = x[...].astype(F32)
+    own = jnp.sum(wide * wide, axis=1, keepdims=True)
+    squares[0] = jnp.broadcast_to(own, (rows, 128))
+    greet(sp, tp)
+    swap_squares = remote(squares.at[0], squares.at[1], sq_sem.at[0], sq_sem.at[1], tp=other)
+    swap_squares.start()
+    swap_squares.wait()
+    total = own + squares[1][:, :1]
+    scale = lax.rsqrt(total / (half * tp) + EPS)
+    home = lax.div(s, per_half) == t
+
+    def slice_send(i):
+        j = t * per_half + i
+        return remote(normed.at[i], blocks.at[s], a_send.at[i], a_recv.at[s], sp=j)
+
+    for i in range(per_half):
+        cols = slice(i * width, (i + 1) * width)
+        normed[i] = (x[:, cols].astype(F32) * scale * gain[t, :, cols]).astype(BF)
+
+        @pl.when(t * per_half + i != s)
+        def _():
+            slice_send(i).start()
+
+        @pl.when(t * per_half + i == s)
+        def _():
+            keep = pltpu.make_async_copy(normed.at[i], blocks.at[s], l_sem)
+            keep.start()
+            keep.wait()
+
+    def forward(b):
+        return remote(blocks.at[b], blocks.at[b], f_send.at[b], a_recv.at[b], tp=other)
+
+    @pl.when(home)
+    def _():
+        forward(s).start()
+
+    low = jnp.zeros((rank, rows), F32)
+    for i in range(per_half):
+        low += columns_dot(down[t, :, i * width : (i + 1) * width], normed[i])
+    note[s, t, :rank] = low
+    note[s, t, rank:] = fade[...]
+
+    def note_send(n):
+        where = {"sp": lax.rem(s + n // tp, sp), "tp": lax.rem(t + n % tp, tp)}
+        return remote(note.at[s, t], note.at[s, t], n_send.at[n], n_recv.at[s, t], **where)
+
+    def right(group, sems, b, d):
+        return remote(group[0].at[b, d], group[1].at[b, d], sems[0].at[b, d], sems[1].at[b, d], sp=after)
+
+    def left(group, sems, b, d):
+        return remote(group[0].at[b, d], group[2].at[b, d], sems[2].at[b, d], sems[3].at[b, d], sp=ahead)
+
+    def ends(group, sems, b):
+        @pl.when(s == 0)
+        def _():
+            for d in range(sp - 1, 0, -1):
+                right(group, sems, b, d).start()
+
+        @pl.when(s == sp - 1)
+        def _():
+            for d in range(sp - 1):
+                left(group, sems, b, d).start()
+
+    def place(k):
+        return lax.rem(s + jnp.where(s < (sp + 1) // 2, k, sp - k), sp)
+
+    for i in (3, 4, 5):
+        loads[i].wait()
+
+    def project_linear(k, carry):
+        b = place(k)
+
+        @pl.when(jnp.logical_or(jnp.logical_not(home), b != s))
+        def _():
+            forward(b).wait_recv()
+
+        @pl.when(jnp.logical_and(home, b != s))
+        def _():
+            forward(b).start()
+
+        block = blocks[b]
+        for d in range(sp):
+            at = 0
+            for i in (3, 4, 5):
+                w = widths[i]
+                lin[0][b, d, :, at : at + w] = dot(block, weights[i][:, d * w : (d + 1) * w]).astype(BF)
+                at += w
+        ends(lin, lin_sem, b)
+        return carry
+
+    lax.fori_loop(0, sp, project_linear, 0)
+    for n in range(1, sp * tp):
+        note_send(n).start()
+    for i in (0, 1, 2):
+        loads[i].wait()
+
+    def relay(group, sems, k):
+        br, bl = k, sp - 1 - k
+        for n in range(sp - 1):
+            dr, dl = sp - 1 - n, n
+
+            @pl.when(jnp.logical_and(s > 0, s < dr))
+            def _():
+                right(group, sems, br, dr).wait_recv()
+                group[0][br, dr] = (
+                    group[0][br, dr].astype(F32) + group[1][br, dr].astype(F32)
+                ).astype(BF)
+                right(group, sems, br, dr).start()
+
+            @pl.when(jnp.logical_and(s < sp - 1, s > dl))
+            def _():
+                left(group, sems, bl, dl).wait_recv()
+                group[0][bl, dl] = (
+                    group[0][bl, dl].astype(F32) + group[2][bl, dl].astype(F32)
+                ).astype(BF)
+                left(group, sems, bl, dl).start()
+
+    def project_window(k, carry):
+        b = place(k)
+        block = blocks[b]
+        keys = dot(block, weights[1][...])
+        vals = dot(block, weights[2][...])
+        qw, kw, vw = widths[:3]
+        for d in range(sp):
+            win[0][b, d, :, :qw] = dot(block, weights[0][:, d * qw : (d + 1) * qw]).astype(BF)
+            win[0][b, d, :, qw : qw + kw] = keys[:, d * kw : (d + 1) * kw].astype(BF)
+            win[0][b, d, :, qw + kw :] = vals[:, d * vw : (d + 1) * vw].astype(BF)
+        ends(win, win_sem, b)
+        relay(lin, lin_sem, k)
+        return carry
+
+    lax.fori_loop(0, sp, project_window, 0)
+
+    def finish(group, sems, b):
+        group[3][b] = group[0][b, s]
+
+        @pl.when(s > 0)
+        def _():
+            right(group, sems, b, s).wait_recv()
+            group[3][b] = (group[3][b].astype(F32) + group[1][b, s].astype(F32)).astype(BF)
+
+        @pl.when(s < sp - 1)
+        def _():
+            left(group, sems, b, s).wait_recv()
+            group[3][b] = (group[3][b].astype(F32) + group[2][b, s].astype(F32)).astype(BF)
+
+    def sent(group, sems, b):
+        for d in range(sp):
+
+            @pl.when(s < d)
+            def _():
+                right(group, sems, b, d).wait_send()
+
+            @pl.when(s > d)
+            def _():
+                left(group, sems, b, d).wait_send()
+
+    def gather_right(held, sems, b, src):
+        ref = held.at[b, src]
+        return remote(ref, ref, sems[0].at[b, src], sems[1].at[b, src], sp=after)
+
+    def gather_left(held, sems, b, src):
+        ref = held.at[b, src]
+        return remote(ref, ref, sems[2].at[b, src], sems[3].at[b, src], sp=ahead)
+
+    def start_own(held, sems, b):
+        @pl.when(s < sp - 1)
+        def _():
+            gather_right(held, sems, b, s).start()
+
+        @pl.when(s > 0)
+        def _():
+            gather_left(held, sems, b, s).start()
+
+    def pass_on(held, sems, b):
+        for n in range(1, sp):
+
+            @pl.when(s - n >= 0)
+            def _():
+                src = jnp.maximum(s - n, 0)
+                gather_right(held, sems, b, src).wait_recv()
+
+                @pl.when(s < sp - 1)
+                def _():
+                    gather_right(held, sems, b, src).start()
+
+            @pl.when(s + n < sp)
+            def _():
+                src = jnp.minimum(s + n, sp - 1)
+                gather_left(held, sems, b, src).wait_recv()
+
+                @pl.when(s > 0)
+                def _():
+                    gather_left(held, sems, b, src).start()
+
+    loads[8].wait()
+    for n in range(1, sp * tp):
+        ps, pt = lax.rem(s + n // tp, sp), lax.rem(t + n % tp, tp)
+        remote(note.at[ps, pt], note.at[ps, pt], n_send.at[n], n_recv.at[ps, pt], tp=other).wait_recv()
+    lk = LOOKUP_FEATURES
+    lane = pl.ds(pl.multiple_of(s * lk, lk), lk)
+    up_own = jnp.concatenate([up[:, lane], jnp.zeros((rows - rank, lk), BF)], axis=0)
+    bias_own = bias[:, lane]
+    row_at = lax.broadcasted_iota(jnp.int32, (rows, rows), 0)
+    col_at = lax.broadcasted_iota(jnp.int32, (rows, rows), 1)
+    span_low = jnp.logical_and(row_at >= col_at, row_at // SPAN == col_at // SPAN)
+    ones_low = jnp.where(span_low, 1.0, 0.0)
+    noted = note.shape[2]
+
+    def linear(b, state):
+        finish(lin, lin_sem, b)
+        rank_rows = note[b, 0, :rank] + note[b, 1, :rank]
+        tall = jnp.concatenate(
+            [rank_rows, note[b, t, rank:], jnp.zeros((rows - noted, rows), F32)], axis=0
+        ).T
+        energies = dot(tall.astype(BF), up_own) + bias_own
+        soft = jnp.minimum(energies, 0.0) - jnp.log1p(jnp.exp(-jnp.abs(energies)))
+        extra = jnp.sum(jnp.where(col_at == rank + s, tall, 0.0), axis=1, keepdims=True)
+        fading = soft / FADING_SOFTNESS + extra
+        running = lax.dot_general(
+            ones_low,
+            fading,
+            (((1,), (0,)), ((), ())),
+            precision=HIGH_PRECISION,
+            preferred_element_type=F32,
+        )
+        query = lin[3][b, :, :lk].astype(F32) * lk ** (-0.5)
+        key = lin[3][b, :, lk : 2 * lk].astype(F32)
+        value = lin[3][b, :, 2 * lk :]
+        decayed = (query * jnp.exp(running)).astype(BF)
+        inner = columns_dot(decayed, (key * jnp.exp(-running)).astype(BF))
+        inner = jnp.where(span_low, inner, 0.0).astype(BF)
+        within = dot(inner, value)
+        carried = []
+        for j in range(rows // SPAN):
+            cut = slice(j * SPAN, (j + 1) * SPAN)
+            end = running[(j + 1) * SPAN - 1 : (j + 1) * SPAN]
+            ending = (key[cut] * jnp.exp(end - running[cut])).astype(BF)
+            carried.append(columns_dot(decayed[cut], state.astype(BF)))
+            state = state * jnp.exp(end) + lax.dot_general(
+                value[cut], ending, (((0,), (0,)), ((), ())), preferred_element_type=F32
+            )
+        flat = within + jnp.concatenate(carried, axis=0)
+        normal = flat * lax.rsqrt(jnp.mean(flat * flat, axis=-1, keepdims=True) + EPS) * head_gain[...]
+        held_g[b, s] = normal.astype(BF)
+        start_own(held_g, g_sem, b)
+        return state
+
+    lax.fori_loop(0, sp, linear, start[...].T)
+
+    def relay_window(k, carry):
+        relay(win, win_sem, k)
+        pass_on(held_g, g_sem, k)
+        return carry
+
+    lax.fori_loop(0, sp, relay_window, 0)
+
+    def finish_window(b, carry):
+        finish(win, win_sem, b)
+        return carry
+
+    lax.fori_loop(0, sp, finish_window, 0)
+    query_at = lax.broadcasted_iota(jnp.int32, (rows, 2 * rows), 0)
+    key_at = lax.broadcasted_iota(jnp.int32, (rows, 2 * rows), 1)
+    distance = query_at - key_at + rows
+    near_by = jnp.logical_and(distance >= 0, distance < WINDOW)
+    far = distance.astype(F32)
+    heads = widths[0] // HD
+    qw = widths[0]
+    for b in order:
+        present = win[3][b]
+        earlier = win[3][max(b - 1, 0)]
+        keys = jnp.concatenate([earlier[:, qw : qw + HD], present[:, qw : qw + HD]], axis=0)
+        vals = jnp.concatenate([earlier[:, qw + HD :], present[:, qw + HD :]], axis=0)
+        allowed = near_by if b else jnp.logical_and(near_by, key_at >= rows)
+        results = []
+        for h in range(heads):
+            number = ((t * sp + s) * heads + h + 1).astype(F32)
+            slope = jnp.exp2(jnp.full((rows, 1), -8.0 / QH, F32) * number)
+            score = columns_dot(present[:, h * HD : (h + 1) * HD], keys) * HD ** (-0.5) - slope * far
+            weight = jnp.where(allowed, jnp.exp(score), 0.0)
+            floor = jnp.exp(jnp.full((rows, 1), sink[s * heads + h], F32))
+            probs = (weight / (jnp.sum(weight, axis=1, keepdims=True) + floor)).astype(BF)
+            results.append(dot(probs, vals))
+        held_n[b, s] = jnp.concatenate(results, axis=1).astype(BF)
+        start_own(held_n, h_sem, b)
+
+    loads[6].wait()
+    loads[7].wait()
+    part = rows // tp
+    near_cols, gated_cols = held_n.shape[3], held_g.shape[3]
+
+    def swap(b):
+        return remote(term.at[b, other], away.at[b], t_send.at[b], t_recv.at[b], tp=other)
+
+    def deliver(b):
+        return remote(term.at[b, t], landed.at[s], o_send.at[b], o_recv.at[s], sp=b)
+
+    def close(b):
+        swap(b).wait()
+        term[b, t] = (term[b, t].astype(F32) + away[b].astype(F32)).astype(BF)
+
+        @pl.when(s != b)
+        def _():
+            deliver(b).start()
+
+        @pl.when(s == b)
+        def _():
+            landed[b] = term[b, t]
+
+    for k, b in enumerate(order):
+        pass_on(held_n, h_sem, b)
+        if k:
+            close(order[k - 1])
+        total = None
+        for src in range(sp):
+            piece = dot(held_n[b, src], weights[6][src * near_cols : (src + 1) * near_cols]) + dot(
+                held_g[b, src], weights[7][src * gated_cols : (src + 1) * gated_cols]
+            )
+            total = piece if total is None else total + piece
+        for h in range(tp):
+            term[b, h] = total[h * part : (h + 1) * part].astype(BF)
+        swap(b).start()
+    close(order[-1])
+
+    def drain(b, carry):
+        sent(lin, lin_sem, b)
+        sent(win, win_sem, b)
+
+        @pl.when(home)
+        def _():
+            forward(b).wait_send()
+
+        for held, sems in ((held_g, g_sem), (held_n, h_sem)):
+            for src in range(sp):
+
+                @pl.when(jnp.logical_and(src <= s, s < sp - 1))
+                def _():
+                    gather_right(held, sems, b, src).wait_send()
+
+                @pl.when(jnp.logical_and(src >= s, s > 0))
+                def _():
+                    gather_left(held, sems, b, src).wait_send()
+
+        return carry
+
+    lax.fori_loop(0, sp, drain, 0)
+    for i in range(per_half):
+
+        @pl.when(t * per_half + i != s)
+        def _():
+            slice_send(i).wait_send()
+
+    for n in range(1, sp * tp):
+        note_send(n).wait_send()
+    columns = landed.shape[2]
+    for b in range(sp):
+
+        @pl.when(s != b)
+        def _():
+            deliver(b).wait_send()
+            remote(landed.at[b], landed.at[b], o_send.at[b], o_recv.at[b], tp=other).wait_recv()
+
+        out[:, b * columns : (b + 1) * columns] = landed[b]
+
+
+def stationary(
+    activations,
+    input_norm_gain,
+    window_query_weight,
+    window_key_weight,
+    window_value_weight,
+    linear_query_weight,
+    linear_key_weight,
+    linear_value_weight,
+    decay_down_factor,
+    decay_up_factor,
+    decay_offset_bias,
+    extra_fading_exponent,
+    starting_state,
+    head_sink_logit,
+    linear_head_gain,
+    window_output_weight,
+    linear_output_weight,
+):
+    sp, tp = lax.axis_size("sp"), lax.axis_size("tp")
+    rows, half = activations.shape
+    matrices = (
+        window_query_weight,
+        window_key_weight,
+        window_value_weight,
+        linear_query_weight,
+        linear_key_weight,
+        linear_value_weight,
+        window_output_weight,
+        linear_output_weight,
+    )
+    widths = tuple(m.shape[1] // sp for m in matrices[:6])
+    wide_window, wide_linear = sum(widths[:3]), sum(widths[3:])
+    rank = decay_down_factor.shape[1]
+    heads_tp = extra_fading_exponent.shape[1]
+    gain = input_norm_gain.reshape(tp, 1, half)
+    down = decay_down_factor.T.reshape(rank, tp, half).transpose(1, 0, 2)
+    fade = jnp.pad(extra_fading_exponent.T, ((0, -heads_tp % 8), (0, 0)))
+    noted = rank + fade.shape[0]
+    columns = window_output_weight.shape[1]
+    order = sorted(range(sp), key=lambda b: -abs(2 * b - sp + 1))
+    vmem = pl.BlockSpec(memory_space=pltpu.VMEM)
+    hbm = pl.BlockSpec(memory_space=pltpu.HBM)
+    dma = pltpu.SemaphoreType.DMA
+    slice_width = half * tp // sp
+
+    def chunks(cols):
+        return [pltpu.VMEM((sp, sp, rows, cols), BF)] * 3 + [pltpu.VMEM((sp, rows, cols), BF)]
+
+    return pl.pallas_call(
+        functools.partial(mixer_kernel, sp, tp, widths, order),
+        out_shape=jax.ShapeDtypeStruct((rows // tp, columns * sp), BF),
+        in_specs=[vmem] * 6
+        + [pl.BlockSpec(memory_space=pltpu.SMEM), vmem]
+        + [hbm] * 9,
+        out_specs=vmem,
+        scratch_shapes=[pltpu.VMEM(m.shape, BF) for m in matrices]
+        + [
+            pltpu.VMEM(starting_state.shape[1:], F32),
+            pltpu.VMEM((2, rows, 128), F32),
+            pltpu.VMEM((sp // tp, rows, slice_width), BF),
+            pltpu.VMEM((sp, rows, slice_width), BF),
+            pltpu.VMEM((sp, tp, noted, rows), F32),
+            pltpu.VMEM((sp, tp, rows // tp, columns), BF),
+            pltpu.VMEM((sp, rows // tp, columns), BF),
+            pltpu.VMEM((sp, rows // tp, columns), BF),
+        ]
+        + chunks(wide_linear)
+        + chunks(wide_window)
+        + [
+            pltpu.VMEM((sp, sp, rows, widths[5]), BF),
+            pltpu.VMEM((sp, sp, rows, widths[0]), BF),
+            dma((9,)),
+            dma((2,)),
+            dma((sp // tp,)),
+            dma((sp,)),
+            dma((sp,)),
+            dma,
+            dma((sp * tp,)),
+            dma((sp, tp)),
+        ]
+        + [dma((sp, sp))] * 16
+        + [dma((sp,))] * 4,
+        compiler_params=pltpu.CompilerParams(
+            collective_id=0, has_side_effects=True, vmem_limit_bytes=56 * 2**20
+        ),
+    )(
+        activations,
+        gain,
+        down,
+        fade,
+        decay_up_factor,
+        decay_offset_bias.reshape(1, -1),
+        head_sink_logit,
+        linear_head_gain.reshape(1, -1),
+        *matrices,
+        starting_state,
+    )
+
+
+def mixer(*arrays):
+    sp, tp = lax.axis_size("sp"), lax.axis_size("tp")
+    rows = arrays[0].shape[0]
+    one_each = KVH == GATED_MIXERS == sp * tp and QH % KVH == 0
+    if tp == 2 and sp % tp == 0 and one_each and rows == WINDOW and rows % SPAN == 0:
+        return stationary(*arrays)
+    return local(*arrays)
+
+
 def solution(mesh):
     placed = (
         P(("fs", "sp"), "tp"),
@@ -249,5 +789,5 @@
         P("tp", "sp"),
     )
     return jax.shard_map(
-        local, mesh=mesh, in_specs=placed, out_specs=P(("fs", "sp", "tp"), None), check_vma=False
-    )
+        mixer, mesh=mesh, in_specs=placed, out_specs=P(("fs", "sp", "tp"), None), check_vma=False
+    )

time: 923 us -> 165 us (0.18)
  waiting for transfers between devices: 845 us -> 0 us
  Pallas kernels: 0 us -> 158 us
  matrix products: 41.2 us -> 0 us
  between operations: 13.7 us -> 0.01 us
  blocking collectives: 9.38 us -> 0 us
    all_gather x10 -> x0, waiting for transfers between devices: 832 us -> none  [the longest x1 146 us: local(): lax.all_gather(matrices[5], 'sp', axis=0, tiled=True)]
    pallas_call x0 -> x1, Pallas kernels: none -> 158 us  [stationary(): pl.pallas_call(functools.partial(mixer_kernel, sp, tp, widths, order), ou...]
    dot_general x18 -> x0, matrix products: 41.2 us -> none  [the longest x6 19.4 us: local(): jnp.dot(normed, segment, preferred_element_type=jnp.float32)]
    all_gather x1 -> x0, blocking collectives: 9.38 us -> none  [prefix(): lax.all_gather(part.astype(kind), axis)]
  transfers between devices with their start and end apart: 12 -> 0, of which waited for: 11 -> 0; matrix products, arithmetic and copies ran while one was open for 5% -> 0% of each run, Pallas kernels for 0% -> 0%
where the time goes in v3:
time: 165 us; the launch traced here: 163 us
  Pallas kernels  158 us (96%)
  local copies, waits for them, and re-layouts  4.71 us (3%)
    pallas_call x1, Pallas kernels, stationary(): pl.pallas_call(functools.partial(mixer_kernel, sp, tp, widths, order), ou...  158 us

profile of v3, /device:TPU:0, one launch (start us, length us, event | category | flops | bytes accessed | tf_op | source)
XLA Modules:
  0.0 162.8 jit_solution(9853620554770416380)
XLA Ops:
  0.0 1.3 pad.4.refs_3_
  1.3 1.6 copy.21
  2.8 158.1 %shard_map.163 = bf16[64,4096]{1,0:T(8,128)(2,1)} custom-call(bf16[128,2048]{1,0:T(8,128)(2,1)} %refs_0_.1, f32[2,1,2048]{2,1,0:T(1,128)} %bitcast.14, bf16[2,16,2048]{2,1,0:T(8,128)(2,1)} %bitcast.12, f32[8,128]{1,0:T(8,128)} %pad.4.refs_3_, bf16[16,512]{1,0:T(8,128)(2,1)} %refs_4_.1, f32[1,512]{1,0:T(1,128)} %bitcast.16, f32[16]{0:T(128)} %refs_6_.1, ...), custom_call_target="tpu_custom_call" | custom-call | tf_op jit(solution)/shard_map/pallas_call | solution.py:711
  160.9 1.9 %copy.23 = bf16[64,4096]{1,0:T(8,128)(2,1)} copy(bf16[64,4096]{1,0:T(8,128)(2,1)} %shard_map.163) | data formatting | bytes 1048576

commit v4 on v3

--- a/solution.py
+++ b/solution.py
@@ -275,11 +275,10 @@
     weights, start = refs[18:26], refs[26]
     squares, normed, blocks, note, term, away, landed = refs[27:34]
     lin = refs[34:38]
-    win = refs[38:42]
-    held_g, held_n = refs[42:44]
-    w_sem, sq_sem, a_send, a_recv, f_send, l_sem, n_send, n_recv = refs[44:52]
-    lin_sem, win_sem, g_sem, h_sem = refs[52:56], refs[56:60], refs[60:64], refs[64:68]
-    t_send, t_recv, o_send, o_recv = refs[68:72]
+    held_g, held_n = refs[38:40]
+    w_sem, sq_sem, a_send, a_recv, f_send, l_sem, n_send, n_recv = refs[40:48]
+    lin_sem, g_sem, h_sem = refs[48:52], refs[52:56], refs[56:60]
+    t_send, t_recv, o_send, o_recv = refs[60:64]
     s, t = lax.axis_index("sp"), lax.axis_index("tp")
     other = 1 - t
     after, ahead = jnp.minimum(s + 1, sp - 1), jnp.maximum(s - 1, 0)
@@ -359,10 +358,10 @@
     def place(k):
         return lax.rem(s + jnp.where(s < (sp + 1) // 2, k, sp - k), sp)
 
-    for i in (3, 4, 5):
+    for i in range(6):
         loads[i].wait()
 
-    def project_linear(k, carry):
+    def project(k, carry):
         b = place(k)
 
         @pl.when(jnp.logical_or(jnp.logical_not(home), b != s))
@@ -374,20 +373,23 @@
             forward(b).start()
 
         block = blocks[b]
+        keys = dot(block, weights[1][...])
+        vals = dot(block, weights[2][...])
+        kw, vw = widths[1], widths[2]
         for d in range(sp):
             at = 0
-            for i in (3, 4, 5):
+            for i in (3, 4, 5, 0):
                 w = widths[i]
                 lin[0][b, d, :, at : at + w] = dot(block, weights[i][:, d * w : (d + 1) * w]).astype(BF)
                 at += w
+            lin[0][b, d, :, at : at + kw] = keys[:, d * kw : (d + 1) * kw].astype(BF)
+            lin[0][b, d, :, at + kw :] = vals[:, d * vw : (d + 1) * vw].astype(BF)
         ends(lin, lin_sem, b)
         return carry
 
-    lax.fori_loop(0, sp, project_linear, 0)
+    lax.fori_loop(0, sp, project, 0)
     for n in range(1, sp * tp):
         note_send(n).start()
-    for i in (0, 1, 2):
-        loads[i].wait()
 
     def relay(group, sems, k):
         br, bl = k, sp - 1 - k
@@ -410,21 +412,11 @@
                 ).astype(BF)
                 left(group, sems, bl, dl).start()
 
-    def project_window(k, carry):
-        b = place(k)
-        block = blocks[b]
-        keys = dot(block, weights[1][...])
-        vals = dot(block, weights[2][...])
-        qw, kw, vw = widths[:3]
-        for d in range(sp):
-            win[0][b, d, :, :qw] = dot(block, weights[0][:, d * qw : (d + 1) * qw]).astype(BF)
-            win[0][b, d, :, qw : qw + kw] = keys[:, d * kw : (d + 1) * kw].astype(BF)
-            win[0][b, d, :, qw + kw :] = vals[:, d * vw : (d + 1) * vw].astype(BF)
-        ends(win, win_sem, b)
+    def relay_step(k, carry):
         relay(lin, lin_sem, k)
         return carry
 
-    lax.fori_loop(0, sp, project_window, 0)
+    lax.fori_loop(0, sp, relay_step, 0)
 
     def finish(group, sems, b):
         group[3][b] = group[0][b, s]
@@ -501,6 +493,7 @@
     span_low = jnp.logical_and(row_at >= col_at, row_at // SPAN == col_at // SPAN)
     ones_low = jnp.where(span_low, 1.0, 0.0)
     noted = note.shape[2]
+    wide = sum(widths[3:])
 
     def linear(b, state):
         finish(lin, lin_sem, b)
@@ -521,7 +514,7 @@
         )
         query = lin[3][b, :, :lk].astype(F32) * lk ** (-0.5)
         key = lin[3][b, :, lk : 2 * lk].astype(F32)
-        value = lin[3][b, :, 2 * lk :]
+        value = lin[3][b, :, 2 * lk : wide]
         decayed = (query * jnp.exp(running)).astype(BF)
         inner = columns_dot(decayed, (key * jnp.exp(-running)).astype(BF))
         inner = jnp.where(span_low, inner, 0.0).astype(BF)
@@ -537,24 +530,16 @@
             )
         flat = within + jnp.concatenate(carried, axis=0)
         normal = flat * lax.rsqrt(jnp.mean(flat * flat, axis=-1, keepdims=True) + EPS) * head_gain[...]
-        held_g[b, s] = normal.astype(BF)
-        start_own(held_g, g_sem, b)
+        q, r = divmod(order.index(b), 2)
+        held_g[q, s, r * rows : (r + 1) * rows] = normal.astype(BF)
         return state
 
-    lax.fori_loop(0, sp, linear, start[...].T)
-
-    def relay_window(k, carry):
-        relay(win, win_sem, k)
-        pass_on(held_g, g_sem, k)
-        return carry
-
-    lax.fori_loop(0, sp, relay_window, 0)
-
-    def finish_window(b, carry):
-        finish(win, win_sem, b)
-        return carry
-
-    lax.fori_loop(0, sp, finish_window, 0)
+    state = start[...].T
+    for b in range(sp):
+        state = linear(b, state)
+    for q in range(sp // 2):
+        start_own(held_g, g_sem, q)
+
     query_at = lax.broadcasted_iota(jnp.int32, (rows, 2 * rows), 0)
     key_at = lax.broadcasted_iota(jnp.int32, (rows, 2 * rows), 1)
     distance = query_at - key_at + rows
@@ -563,8 +548,8 @@
     heads = widths[0] // HD
     qw = widths[0]
     for b in order:
-        present = win[3][b]
-        earlier = win[3][max(b - 1, 0)]
+        present = lin[3][b, :, wide:]
+        earlier = lin[3][max(b - 1, 0), :, wide:]
         keys = jnp.concatenate([earlier[:, qw : qw + HD], present[:, qw : qw + HD]], axis=0)
         vals = jnp.concatenate([earlier[:, qw + HD :], present[:, qw + HD :]], axis=0)
         allowed = near_by if b else jnp.logical_and(near_by, key_at >= rows)
@@ -577,8 +562,10 @@
             floor = jnp.exp(jnp.full((rows, 1), sink[s * heads + h], F32))
             probs = (weight / (jnp.sum(weight, axis=1, keepdims=True) + floor)).astype(BF)
             results.append(dot(probs, vals))
-        held_n[b, s] = jnp.concatenate(results, axis=1).astype(BF)
-        start_own(held_n, h_sem, b)
+        q, r = divmod(order.index(b), 2)
+        held_n[q, s, r * rows : (r + 1) * rows] = jnp.concatenate(results, axis=1).astype(BF)
+        if r:
+            start_own(held_n, h_sem, q)
 
     loads[6].wait()
     loads[7].wait()
@@ -603,14 +590,18 @@
         def _():
             landed[b] = term[b, t]
 
+    for q in range(sp // 2):
+        pass_on(held_g, g_sem, q)
     for k, b in enumerate(order):
-        pass_on(held_n, h_sem, b)
+        q, r = divmod(k, 2)
+        if r == 0:
+            pass_on(held_n, h_sem, q)
         if k:
             close(order[k - 1])
         total = None
         for src in range(sp):
-            piece = dot(held_n[b, src], weights[6][src * near_cols : (src + 1) * near_cols]) + dot(
-                held_g[b, src], weights[7][src * gated_cols : (src + 1) * gated_cols]
+            piece = dot(held_n[q, src, r * rows : (r + 1) * rows], weights[6][src * near_cols : (src + 1) * near_cols]) + dot(
+                held_g[q, src, r * rows : (r + 1) * rows], weights[7][src * gated_cols : (src + 1) * gated_cols]
             )
             total = piece if total is None else total + piece
         for h in range(tp):
@@ -620,26 +611,26 @@
 
     def drain(b, carry):
         sent(lin, lin_sem, b)
-        sent(win, win_sem, b)
 
         @pl.when(home)
         def _():
             forward(b).wait_send()
 
-        for held, sems in ((held_g, g_sem), (held_n, h_sem)):
+        return carry
+
+    lax.fori_loop(0, sp, drain, 0)
+    for held, sems in ((held_g, g_sem), (held_n, h_sem)):
+        for q in range(sp // 2):
             for src in range(sp):
 
                 @pl.when(jnp.logical_and(src <= s, s < sp - 1))
                 def _():
-                    gather_right(held, sems, b, src).wait_send()
+                    gather_right(held, sems, q, src).wait_send()
 
                 @pl.when(jnp.logical_and(src >= s, s > 0))
                 def _():
-                    gather_left(held, sems, b, src).wait_send()
-
-        return carry
-
-    lax.fori_loop(0, sp, drain, 0)
+                    gather_left(held, sems, q, src).wait_send()
+
     for i in range(per_half):
 
         @pl.when(t * per_half + i != s)
@@ -691,7 +682,6 @@
         linear_output_weight,
     )
     widths = tuple(m.shape[1] // sp for m in matrices[:6])
-    wide_window, wide_linear = sum(widths[:3]), sum(widths[3:])
     rank = decay_down_factor.shape[1]
     heads_tp = extra_fading_exponent.shape[1]
     gain = input_norm_gain.reshape(tp, 1, half)
@@ -726,11 +716,10 @@
             pltpu.VMEM((sp, rows // tp, columns), BF),
             pltpu.VMEM((sp, rows // tp, columns), BF),
         ]
-        + chunks(wide_linear)
-        + chunks(wide_window)
+        + chunks(sum(widths))
         + [
-            pltpu.VMEM((sp, sp, rows, widths[5]), BF),
-            pltpu.VMEM((sp, sp, rows, widths[0]), BF),
+            pltpu.VMEM((sp // 2, sp, 2 * rows, widths[5]), BF),
+            pltpu.VMEM((sp // 2, sp, 2 * rows, widths[0]), BF),
             dma((9,)),
             dma((2,)),
             dma((sp // tp,)),
@@ -740,7 +729,7 @@
             dma((sp * tp,)),
             dma((sp, tp)),
         ]
-        + [dma((sp, sp))] * 16
+        + [dma((sp, sp))] * 12
         + [dma((sp,))] * 4,
         compiler_params=pltpu.CompilerParams(
             collective_id=0, has_side_effects=True, vmem_limit_bytes=56 * 2**20

time: 165 us -> 155 us (0.939); the launches traced: 163 us -> 155 us
  Pallas kernels: 158 us -> 150 us
    pallas_call x1, Pallas kernels: 158 us -> 150 us  [stationary(): pl.pallas_call(functools.partial(mixer_kernel, sp, tp, widths, order), ou...]
where the time goes in v4:
time: 155 us
  Pallas kernels  150 us (97%)
  local copies, waits for them, and re-layouts  4.71 us (3%)
    pallas_call x1, Pallas kernels, stationary(): pl.pallas_call(functools.partial(mixer_kernel, sp, tp, widths, order), ou...  150 us

profile of v4, /device:TPU:0, one launch (start us, length us, event | category | flops | bytes accessed | tf_op | source)
XLA Modules:
  0.0 155.2 jit_solution(6618242907734270126)
XLA Ops:
  0.0 1.3 pad.4.refs_3_
  1.3 1.6 %copy.21 = bf16[2,2,8,2048]{3,2,0,1:T(8,128)(2,1)} copy(bf16[2,2,8,2048]{3,2,1,0:T(8,128)(2,1)} %bitcast.13) | data formatting | bytes 262144 | tf_op jit(solution)/shard_map/reshape | solution.py:688
  2.8 150.4 %shard_map.163 = bf16[64,4096]{1,0:T(8,128)(2,1)} custom-call(bf16[128,2048]{1,0:T(8,128)(2,1)} %refs_0_.1, f32[2,1,2048]{2,1,0:T(1,128)} %bitcast.14, bf16[2,16,2048]{2,1,0:T(8,128)(2,1)} %bitcast.12, f32[8,128]{1,0:T(8,128)} %pad.4.refs_3_, bf16[16,512]{1,0:T(8,128)(2,1)} %refs_4_.1, f32[1,512]{1,0:T(1,128)} %bitcast.16, f32[16]{0:T(128)} %refs_6_.1, ...), custom_call_target="tpu_custom_call" | custom-call | tf_op jit(solution)/shard_map/pallas_call | solution.py:701
  153.3 1.9 %copy.23 = bf16[64,4096]{1,0:T(8,128)(2,1)} copy(bf16[64,4096]{1,0:T(8,128)(2,1)} %shard_map.163) | data formatting | bytes 1048576

commit v5 on v4

--- a/solution.py
+++ b/solution.py
@@ -344,16 +344,30 @@
     def left(group, sems, b, d):
         return remote(group[0].at[b, d], group[2].at[b, d], sems[2].at[b, d], sems[3].at[b, d], sp=ahead)
 
-    def ends(group, sems, b):
-        @pl.when(s == 0)
-        def _():
-            for d in range(sp - 1, 0, -1):
-                right(group, sems, b, d).start()
-
-        @pl.when(s == sp - 1)
-        def _():
-            for d in range(sp - 1):
-                left(group, sems, b, d).start()
+    def ends(group, sems, k):
+        for n in range(2):
+
+            @pl.when(jnp.logical_and(s == 0, k == 0))
+            def _():
+                right(group, sems, 0, sp - 1 - n).start()
+
+            @pl.when(jnp.logical_and(s == sp - 1, k == 0))
+            def _():
+                left(group, sems, sp - 1, n).start()
+
+    def paced(group, sems, k, n):
+        ready = k >= 0 if n > 1 else k >= 1
+        k_old, n_old = (k, n - 2) if n > 1 else (k - 1, n + sp - 3)
+
+        @pl.when(jnp.logical_and(s == 0, ready))
+        def _():
+            right(group, sems, k_old, sp - 1 - n_old).wait_send()
+            right(group, sems, k, sp - 1 - n).start()
+
+        @pl.when(jnp.logical_and(s == sp - 1, ready))
+        def _():
+            left(group, sems, sp - 1 - k_old, n_old).wait_send()
+            left(group, sems, sp - 1 - k, n).start()
 
     def place(k):
         return lax.rem(s + jnp.where(s < (sp + 1) // 2, k, sp - k), sp)
@@ -384,7 +398,7 @@
                 at += w
             lin[0][b, d, :, at : at + kw] = keys[:, d * kw : (d + 1) * kw].astype(BF)
             lin[0][b, d, :, at + kw :] = vals[:, d * vw : (d + 1) * vw].astype(BF)
-        ends(lin, lin_sem, b)
+        ends(lin, lin_sem, k)
         return carry
 
     lax.fori_loop(0, sp, project, 0)
@@ -395,6 +409,7 @@
         br, bl = k, sp - 1 - k
         for n in range(sp - 1):
             dr, dl = sp - 1 - n, n
+            paced(group, sems, k, n)
 
             @pl.when(jnp.logical_and(s > 0, s < dr))
             def _():
@@ -433,12 +448,14 @@
 
     def sent(group, sems, b):
         for d in range(sp):
-
-            @pl.when(s < d)
+            last_right = jnp.logical_or(s > 0, jnp.logical_and(b == sp - 1, d <= 2))
+            last_left = jnp.logical_or(s < sp - 1, jnp.logical_and(b == 0, d >= sp - 3))
+
+            @pl.when(jnp.logical_and(s < d, last_right))
             def _():
                 right(group, sems, b, d).wait_send()
 
-            @pl.when(s > d)
+            @pl.when(jnp.logical_and(s > d, last_left))
             def _():
                 left(group, sems, b, d).wait_send()
 

time: 155 us -> 153 us (0.987)
    pallas_call x1, Pallas kernels: 150 us -> 149 us  [stationary(): pl.pallas_call(functools.partial(mixer_kernel, sp, tp, widths, order), ou...]
where the time goes in v5:
time: 153 us
  Pallas kernels  149 us (97%)
  local copies, waits for them, and re-layouts  4.71 us (3%)
    pallas_call x1, Pallas kernels, stationary(): pl.pallas_call(functools.partial(mixer_kernel, sp, tp, widths, order), ou...  149 us

profile of v5, /device:TPU:0, one launch (start us, length us, event | category | flops | bytes accessed | tf_op | source)
XLA Modules:
  0.0 153.2 jit_solution(1297336828763055876)
XLA Ops:
  0.0 1.3 pad.4.refs_3_
  1.3 1.6 %copy.21 = bf16[2,2,8,2048]{3,2,0,1:T(8,128)(2,1)} copy(bf16[2,2,8,2048]{3,2,1,0:T(8,128)(2,1)} %bitcast.13) | data formatting | bytes 262144 | tf_op jit(solution)/shard_map/reshape | solution.py:705
  2.8 148.5 %shard_map.163 = bf16[64,4096]{1,0:T(8,128)(2,1)} custom-call(bf16[128,2048]{1,0:T(8,128)(2,1)} %refs_0_.1, f32[2,1,2048]{2,1,0:T(1,128)} %bitcast.14, bf16[2,16,2048]{2,1,0:T(8,128)(2,1)} %bitcast.12, f32[8,128]{1,0:T(8,128)} %pad.4.refs_3_, bf16[16,512]{1,0:T(8,128)(2,1)} %refs_4_.1, f32[1,512]{1,0:T(1,128)} %bitcast.16, f32[16]{0:T(128)} %refs_6_.1, ...), custom_call_target="tpu_custom_call" | custom-call | tf_op jit(solution)/shard_map/pallas_call | solution.py:718
  151.4 1.9 %copy.23 = bf16[64,4096]{1,0:T(8,128)(2,1)} copy(bf16[64,4096]{1,0:T(8,128)(2,1)} %shard_map.163) | data formatting | bytes 1048576
